TPU v7x, 512 devices: a whole 4x8x8 slice. The times are simulated.
512 devices in a mesh: sp: 64 (over z, y), tp: 8 (over x, core).
Axes of the slice: x: 4, y: 8, z: 8, core: 2. Of those that a mesh axis runs over, the one named last changes fastest.
Arguments:
- tokens: bfloat16 [49152, 2048], P(('sp', 'tp')), may hold values from -6 to 6
- input_norm_gain: bfloat16 [2048], replicated, may hold values from 0.099609375 to 1.8984375
- convolution_outer_weight: bfloat16 [2048, 1024], P(None, 'tp'), may hold values from -0.125 to 0.125
- convolution_inner_weight: bfloat16 [2048, 1024], P(None, 'tp'), may hold values from -0.125 to 0.125
- convolution_signal_weight: bfloat16 [2048, 1024], P(None, 'tp'), may hold values from -0.125 to 0.125
- convolution_kernel_taps: bfloat16 [3, 1024], replicated, may hold values from -3.5 to 3.5
- memory_query_matrix: bfloat16 [2048, 512], P(None, 'tp'), may hold values from -0.125 to 0.125
- memory_key_matrix: bfloat16 [2048, 512], P(None, 'tp'), may hold values from -0.125 to 0.125
- memory_value_matrix: bfloat16 [2048, 1024], P(None, 'tp'), may hold values from -0.125 to 0.125
- output_gate_weight: bfloat16 [2048, 1024], P(None, 'tp'), may hold values from -0.125 to 0.125
- input_gate_weight: bfloat16 [2048, 8], replicated, may hold values from -0.5 to 0.5
- forget_gate_weight: bfloat16 [2048, 8], replicated, may hold values from -0.125 to 0.125
- input_gate_bias: float32 [8], replicated, may hold values from -1 to 125
- forget_gate_bias: float32 [8], replicated, may hold values from 3.5 to 12.5
- position_forget_factor: float32 [49152], P('sp'), may hold values from 0.5 to 2
- extra_log_decay: float32 [49152, 8], P('sp'), may hold values from -0.7 to 0
- starting_memory_state: float32 [8, 64, 128], replicated, may hold values from -6 to 6
- starting_log_scale: float32 [8], replicated, may hold values from 5 to 125
- head_norm_gain: bfloat16 [1024], replicated, may hold values from 0.099609375 to 1.8984375
- convolution_output_weight: bfloat16 [1024, 2048], P('tp'), may hold values from -0.125 to 0.125
- memory_output_weight: bfloat16 [1024, 2048], P('tp'), may hold values from -0.125 to 0.125
Outputs:
- mixed: bfloat16 [49152, 2048], P(('sp', 'tp'))
All inputs are finite; a program needn't handle non-finite values.
Results may differ from a plain program's by a relative error of at most 0.035.
Values may be sent and summed in bfloat16 or wider, within the bound.
No kernel may reach another device: no remote copies, remote signals or barrier semaphores. Data moves between devices by JAX's collectives and lax.ppermute only.
A program may use at most 64 MiB of HBM per device.

v0:
```python
import functools

import jax
import jax.numpy as jnp
from jax import lax
from jax.experimental import pallas as pl
from jax.experimental.pallas import tpu as pltpu
from jax.sharding import PartitionSpec as P


DQK = 64
DV = 128
EPS = 1e-06
FLOOR = -1e30
F32 = jnp.float32
BF16 = jnp.bfloat16
PAYLOAD = 80

SPACES = {
    "vmem": (pltpu.VMEM, pltpu.VMEM),
    "hbm": (pltpu.HBM, pltpu.HBM),
    "load": (pltpu.HBM, pltpu.VMEM),
    "smem": (pltpu.HBM, pltpu.SMEM),
}


def call(body, outs, ins, scratch=(), flops=10**8, limit=16 << 20):
    results = pl.pallas_call(
        body,
        out_shape=tuple(SPACES[how][0](shape, kind) for how, shape, kind in outs),
        in_specs=[pl.BlockSpec(memory_space=SPACES[how][1]) for how, _ in ins],
        out_specs=tuple(pl.BlockSpec(memory_space=SPACES[how][1]) for how, _, _ in outs),
        scratch_shapes=list(scratch),
        compiler_params=pltpu.CompilerParams(vmem_limit_bytes=limit),
        cost_estimate=pl.CostEstimate(flops=flops, bytes_accessed=1 << 20, transcendentals=0),
    )(*[pltpu.with_memory_space_constraint(array, SPACES[how][0]) for how, array in ins])
    return results[0] if len(outs) == 1 else results


def tag(how, *arrays):
    return [(how, array) for array in arrays]


def dot(a, b, dims=((1,), (0,))):
    return lax.dot_general(a, b, (dims, ((), ())), preferred_element_type=F32)


def norm_body(tokens, gain, out):
    wide = tokens[...].astype(F32)
    scale = lax.rsqrt(jnp.mean(wide * wide, axis=1, keepdims=True) + EPS)
    out[...] = (wide * scale * gain[...].astype(F32).reshape(1, 2048)).astype(BF16)


def own_tp():
    return lax.axis_index("tp").astype(jnp.int32)


def own_sp():
    return lax.axis_index("sp").astype(jnp.int32)


def places(tp):
    x, core = tp // 2, tp % 2
    return [
        ((x + shift) % 4) * 2 + (1 - core if swapped else core)
        for swapped in (0, 1)
        for shift in (0, 3, 1, 2)
    ]


def stack_body(b0, b1, b2, out):
    out[0:96, :] = b0[...]
    out[96:192, :] = b1[...]
    out[192:288, :] = b2[...]


def split3(value):
    high = value.astype(BF16).astype(F32)
    rest = value - high
    middle = rest.astype(BF16).astype(F32)
    return [high, middle, rest - middle]


def lane_scan(value, op, neutral):
    lane = lax.broadcasted_iota(jnp.int32, value.shape, 1)
    step = 1
    while step < 128:
        value = op(value, jnp.where(lane >= step, pltpu.roll(value, step, 1), neutral))
        step *= 2
    return value


def row_scan(value, op, neutral):
    last = jnp.broadcast_to(value[:, 127:128], value.shape)
    row = lax.broadcasted_iota(jnp.int32, value.shape, 0)
    before = jnp.where(row >= 1, pltpu.roll(last, 1, 0), neutral)
    for step in (1, 2, 4):
        before = op(before, jnp.where(row >= step, pltpu.roll(before, step, 0), neutral))
    return before


def rows_of(wide_row):
    pieces = [wide_row[:, 128 * b : 128 * (b + 1)] for b in range(6)]
    return jnp.concatenate(pieces + [jnp.zeros((2, 128), F32)], axis=0)


def prepare_body(
    in_bias, forget_bias, start_scale, normed, w_key, w_query, w_input, w_forget, w_value,
    w_inner, w_signal, w_conv, w_memory, factor, extra, taps, gain,
    w_turned, w_value_out, w_rim, w_out, aside, sems,
):
    loads = [
        (w_key, w_turned.at[0:64, :]),
        (w_query, w_turned.at[64:128, :]),
        (w_input, w_turned.at[128:136, :]),
        (w_forget, w_turned.at[136:144, :]),
        (w_value, w_value_out),
        (w_inner, w_rim.at[:, 0:128]),
        (w_signal, w_rim.at[:, 128:256]),
        (w_conv, w_out.at[0:128, :]),
        (w_memory, w_out.at[128:256, :]),
    ]
    loads = [pltpu.make_async_copy(a, b, sems.at[i]) for i, (a, b) in enumerate(loads)]
    for load in loads:
        load.start()
    head = own_tp()
    w_turned[144:256, :] = jnp.zeros((112, 2048), BF16)
    aside[0:8, :] = rows_of(factor[...].reshape(1, 768))
    aside[8:16, :] = rows_of(extra[pl.ds(head, 1), :])
    aside[16:24, :] = jnp.full((8, 128), in_bias[head], F32)
    aside[24:32, :] = jnp.full((8, 128), forget_bias[head], F32)
    aside[32:40, :] = jnp.full((8, 128), start_scale[head], F32)
    lanes = pl.ds(pl.multiple_of(head * 128, 128), 128)
    gains = gain[...].astype(F32).reshape(1, 1024)
    own_gain = jnp.zeros((1, 128), F32)
    for i in range(8):
        own_gain = jnp.where(head == i, gains[:, 128 * i : 128 * (i + 1)], own_gain)
    aside[40:48, :] = jnp.concatenate(
        [taps[:, lanes].astype(F32), own_gain, jnp.zeros((4, 128), F32)], axis=0
    )
    for load in loads:
        load.wait()


def state_body(
    b0, b1, b2, b3, twins, b7, w_turned, w_value, w_rim, aside,
    payload, kqv_out, level_out, rows_out, rows, kqv, level_keep, sems,
):
    head = own_tp()
    blocks = [b0, b1, b2, b3] + [twins.at[pl.ds(96 * i, 96), :] for i in range(3)] + [b7]
    for place, block in zip(places(head), blocks):
        rows[pl.ds(pl.multiple_of(place * 96, 32), 96), :] = block[...]
    savings = [
        pltpu.make_async_copy(rows, rows_out, sems.at[0]),
        pltpu.make_async_copy(kqv, kqv_out, sems.at[1]),
        pltpu.make_async_copy(level_keep, level_out, sems.at[2]),
    ]
    savings[0].start()
    first = dot(rows[...], w_turned[...], ((1,), (1,)))
    turned = [jnp.transpose(first[128 * b : 128 * (b + 1), 128:256]) for b in range(6)]
    mine = lax.broadcasted_iota(jnp.int32, (8, 128), 0) == head
    pick = lambda part: jnp.sum(jnp.where(mine, part, 0.0), axis=0, keepdims=True)
    blank = jnp.zeros((2, 128), F32)
    log_input = jnp.concatenate([pick(t[0:8]) for t in turned] + [blank], axis=0) + aside[16:24, :]
    forget = jnp.concatenate([pick(t[8:16]) for t in turned] + [blank], axis=0) + aside[24:32, :]
    log_sig = jnp.minimum(forget, 0.0) - jnp.log1p(jnp.exp(-jnp.abs(forget)))
    log_forget = aside[0:8, :] * log_sig + aside[8:16, :]
    real = lax.broadcasted_iota(jnp.int32, (8, 128), 0) < 6
    until = lax.broadcasted_iota(jnp.int32, (128, 128), 0)
    until = (until <= lax.broadcasted_iota(jnp.int32, (128, 128), 1)).astype(F32)
    cumul = lax.dot_general(
        jnp.where(real, log_forget, 0.0),
        until,
        (((1,), (0,)), ((), ())),
        precision=lax.Precision.HIGHEST,
        preferred_element_type=F32,
    )
    cumul = cumul + row_scan(cumul, jnp.add, 0.0)
    level = jnp.where(real, log_input - cumul, FLOOR)
    total = cumul[5:6, 127:128]
    highest = jnp.max(level, keepdims=True)
    peak = jnp.broadcast_to(total + highest, (1, 128))
    weight = jnp.exp(level - highest)
    columns = jnp.transpose(jnp.concatenate([weight, jnp.zeros((120, 128), F32)], axis=0))
    values = dot(rows[...], w_value[...]).astype(BF16)
    kqv[:, 0:128] = first[:, 0:128].astype(BF16)
    kqv[:, 128:256] = values
    savings[1].start()
    level_keep[...] = level
    savings[2].start()
    pieces = []
    for b in range(6):
        keys = first[128 * b : 128 * (b + 1), 0:DQK].astype(BF16).astype(F32)
        pieces.append((keys * columns[:, b : b + 1]).astype(BF16))
    state = dot(jnp.concatenate(pieces, axis=0), values, ((0,), (0,)))
    rim = dot(rows[752:768, :], w_rim[...])
    packed = jnp.concatenate(
        [state]
        + split3(peak)
        + split3(jnp.broadcast_to(total, (1, 128)))
        + [rim[14:16, 0:128], rim[14:16, 128:256], jnp.zeros((PAYLOAD - 74, 128), F32)],
        axis=0,
    ).astype(BF16)
    for i in range(8):
        payload[i] = packed
    for saving in savings:
        saving.wait()


def local_body(level_in, kqv, local_out, top_out):
    level = level_in[...]
    top = lane_scan(level, jnp.maximum, FLOOR)
    top = jnp.maximum(top, row_scan(top, jnp.maximum, FLOOR))
    tops = jnp.transpose(jnp.concatenate([top, jnp.zeros((120, 128), F32)], axis=0))
    top_out[...] = tops
    row = lax.broadcasted_iota(jnp.int32, (128, 128), 0)
    column = lax.broadcasted_iota(jnp.int32, (128, 128), 1)
    causal = row >= column
    for b in range(6):
        high = 128 * (b + 1)
        query = (kqv[128 * b : high, DQK : 2 * DQK].astype(F32) * DQK**-0.5).astype(BF16)
        scores = dot(query, kqv[0:high, 0:DQK], ((1,), (1,)))
        parts = []
        for u in range(b + 1):
            power = level[u : u + 1, :] - tops[:, b : b + 1]
            if u == b:
                power = jnp.where(causal, power, FLOOR)
            parts.append((scores[:, 128 * u : 128 * (u + 1)] * jnp.exp(power)).astype(BF16))
        weights = parts[0] if b == 0 else jnp.concatenate(parts, axis=1)
        local_out[128 * b : high, :] = dot(weights, kqv[0:high, 128:256])


def mixer_body(
    rows_in, w_outer, w_inner, w_signal, w_gate, aside, before,
    gate_out, conv_out, edge_out, rows, w_one, w_two, sems,
):
    loads = [
        pltpu.make_async_copy(w_outer, w_one.at[:, 0:128], sems.at[0]),
        pltpu.make_async_copy(w_inner, w_one.at[:, 128:256], sems.at[1]),
        pltpu.make_async_copy(rows_in, rows, sems.at[2]),
        pltpu.make_async_copy(w_signal, w_two.at[:, 0:128], sems.at[3]),
        pltpu.make_async_copy(w_gate, w_two.at[:, 128:256], sems.at[4]),
    ]
    for load in loads:
        load.start()
    for load in loads[0:3]:
        load.wait()
    first = dot(rows[...], w_one[...])
    outer = first[:, 0:128].astype(BF16).astype(F32)
    inner = first[:, 128:256].astype(BF16).astype(F32)
    for load in loads[3:5]:
        load.wait()
    second = dot(rows[...], w_two[...])
    signal = second[:, 0:128].astype(BF16).astype(F32)
    gate_out[...] = jax.nn.sigmoid(second[:, 128:256].astype(BF16).astype(F32)).astype(BF16)
    tap = aside[40:43, :]
    mixed = inner * signal
    at = lax.broadcasted_iota(jnp.int32, mixed.shape, 0)
    one = jnp.where(at >= 1, pltpu.roll(mixed, 1, 0), 0.0)
    two = jnp.where(at >= 2, pltpu.roll(mixed, 2, 0), 0.0)
    summed = tap[0:1] * two + tap[1:2] * one + tap[2:3] * mixed
    conv_out[...] = (outer * summed).astype(BF16)
    edge_out[0:16, :] = summed[0:16]
    edge_out[16:32, :] = outer[0:16]


def merged(states, peaks, decays, allowed, upto):
    scales = []
    after = jnp.zeros((1, 128), F32)
    for i in reversed(range(8)):
        scales.append(jnp.where(allowed[i], peaks[i] + after, FLOOR))
        after = after + jnp.where(upto[i], decays[i], 0.0)
    scales = scales[::-1]
    ceiling = functools.reduce(jnp.maximum, scales)
    total = jnp.zeros((DQK, DV), F32)
    for i in range(8):
        factor = jnp.where(allowed[i], jnp.exp(scales[i] - ceiling), 0.0)
        total = total + factor * states[i]
    return total, ceiling, after


def unpack(received):
    wide = [received[i].astype(F32) for i in range(8)]
    return (
        [w[0:64] for w in wide],
        [w[64:65] + w[65:66] + w[66:67] for w in wide],
        [w[67:68] + w[68:69] + w[69:70] for w in wide],
        [w[70:74] for w in wide],
    )


def line_body(received, tops, payload, before):
    me = own_sp() % 8
    states, peaks, decays, rims = unpack(received)
    every = [True] * 8
    state, peak, decay = merged(states, peaks, decays, every, every)
    packed = jnp.concatenate(
        [state] + split3(peak) + split3(decay) + [rims[7], jnp.zeros((PAYLOAD - 74, 128), F32)],
        axis=0,
    ).astype(BF16)
    for i in range(8):
        payload[i] = packed
    earlier = [i < me for i in range(8)]
    state, peak, decay = merged(states, peaks, decays, earlier, earlier)
    rim = jnp.zeros((4, 128), F32)
    for i in range(7):
        rim = jnp.where(me == i + 1, rims[i], rim)
    before[0:64, :] = state
    before[64:72, :] = jnp.concatenate([peak, decay, rim, jnp.zeros((2, 128), F32)], axis=0)


def final_body(
    received, aside, before_in, start_state, local_in, tops_in, gate_in, kqv_in, conv_in, edge_in,
    out, before, first_state, tops, local, out_gate, kqv, conv, edge, sems,
):
    head, y, z = own_tp(), own_sp() % 8, own_sp() // 8
    loads = [
        (start_state.at[head], first_state),
        (before_in, before),
        (tops_in, tops),
        (kqv_in.at[:, 0:128], kqv),
        (local_in, local),
        (gate_in, out_gate),
        (conv_in, conv),
        (edge_in, edge),
    ]
    loads = [pltpu.make_async_copy(a, b, sems.at[i]) for i, (a, b) in enumerate(loads)]
    for load in loads:
        load.start()
    states, peaks, decays, rims = unpack(received)
    earlier = [i < z for i in range(8)]
    state, peak, decay = merged(states, peaks, decays, earlier, earlier)
    lifted = aside[32:33, :] + decay
    ceiling = jnp.maximum(lifted, peak)
    loads[0].wait()
    state = jnp.exp(lifted - ceiling) * first_state[...] + jnp.exp(peak - ceiling) * state
    loads[1].wait()
    lifted = ceiling + before[65:66, :]
    peak = before[64:65, :]
    ceiling = jnp.maximum(lifted, peak)
    state = jnp.exp(lifted - ceiling) * state + jnp.exp(peak - ceiling) * before[0:64, :]
    state = (state * DQK**-0.5).astype(BF16)
    loads[2].wait()
    top = tops[...]
    best = jnp.maximum(top, ceiling)
    keep = jnp.exp(top - best)
    bring = jnp.exp(ceiling - best)
    for load in loads[3:]:
        load.wait()
    scale = aside[43:44, :]
    for b in range(6):
        here = slice(128 * b, 128 * (b + 1))
        remote = dot(kqv[here, DQK : 2 * DQK], state)
        number = bring[:, b : b + 1] * remote + keep[:, b : b + 1] * local[here, :]
        spread = lax.rsqrt(jnp.mean(number * number, axis=1, keepdims=True) + EPS)
        out[here, 128:256] = (number * spread * scale * out_gate[here, :].astype(F32)).astype(BF16)
    out[:, 0:128] = conv[...]
    rim = before[66:70, :]
    for i in range(7):
        rim = jnp.where(jnp.logical_and(y == 0, z == i + 1), rims[i], rim)
    past = rim[0:2] * rim[2:4]
    tap = aside[40:43, :]
    extra = jnp.concatenate(
        [tap[0:1] * past[0:1] + tap[1:2] * past[1:2], tap[0:1] * past[1:2], jnp.zeros((14, 128), F32)],
        axis=0,
    )
    out[0:16, 0:128] = (edge[16:32, :] * (edge[0:16, :] + extra)).astype(BF16)


def project_body(received, w0, w1, w2, w3, sent, kept, weights, sems):
    tp = own_tp()
    x, core = tp // 2, tp % 2
    loads = []
    for n in range(4):
        for i, weight in enumerate((w0, w3)):
            cut = pl.ds(512 * n, 512)
            loads.append(
                pltpu.make_async_copy(
                    weight.at[:, cut], weights.at[pl.ds(256 * i, 256), cut], sems.at[n, i]
                )
            )
    for load in loads:
        load.start()
    there = pl.ds(pl.multiple_of((1 - core) * 96, 32), 96)
    here = pl.ds(pl.multiple_of(core * 96, 32), 96)
    parts = [
        jnp.concatenate([received[(x + shift) % 4, rows, :] for rows in (there, here)], axis=0)
        for shift in (0, 3, 1, 2)
    ]
    for n in range(4):
        cut = slice(512 * n, 512 * (n + 1))
        total = dot(parts[1], w1[:, cut]) + dot(parts[2], w2[:, cut])
        for load in loads[2 * n : 2 * n + 2]:
            load.wait()
        total = total + dot(parts[0], weights[0:256, cut]) + dot(parts[3], weights[256:512, cut])
        sent[:, cut] = total[0:96].astype(BF16)
        kept[:, cut] = total[96:192]


def add_body(one, other, out):
    out[...] = (one[...] + other[...].astype(F32)).astype(BF16)


def tp_moves(move):
    moves = []
    for i in range(8):
        x, core = move(i // 2, i % 2)
        moves.append((i, (x % 4) * 2 + core))
    return moves


UP = tp_moves(lambda x, c: (x + 1, c))
DOWN = tp_moves(lambda x, c: (x - 1, c))
ACROSS = tp_moves(lambda x, c: (x + 2, c))
SWAP = tp_moves(lambda x, c: (x, 1 - c))
X_GROUPS = [[0, 2, 4, 6], [1, 3, 5, 7]]
Y_GROUPS = [[z * 8 + y for y in range(8)] for z in range(8)]
Z_GROUPS = [[z * 8 + y for z in range(8)] for y in range(8)]


def move(value, pairs):
    return lax.ppermute(value, "tp", pairs)


def to_all(copies, groups):
    return lax.all_to_all(copies, "sp", 0, 0, axis_index_groups=groups)


def on_device(
    tokens, input_norm_gain, w_outer, w_inner, w_signal, taps, w_query, w_key, w_value, w_gate,
    w_input, w_forget, in_bias, forget_bias, factor, extra, start_state, start_scale, head_gain,
    w_conv_out, w_memory_out,
):
    normed = call(
        norm_body, [("vmem", (96, 2048), BF16)], tag("load", tokens, input_norm_gain)
    )
    *prepared, w_out, aside = call(
        prepare_body,
        [
            ("vmem", (256, 2048), BF16),
            ("vmem", (2048, 128), BF16),
            ("vmem", (2048, 256), BF16),
            ("vmem", (256, 2048), BF16),
            ("vmem", (48, 128), F32),
        ],
        tag("smem", in_bias, forget_bias, start_scale)
        + tag("vmem", normed)
        + tag("hbm", w_key.T, w_query.T, w_input.T, w_forget.T, w_value, w_inner, w_signal)
        + tag("hbm", w_conv_out, w_memory_out)
        + tag("load", factor, extra.T, taps, head_gain),
        [pltpu.SemaphoreType.DMA((9,))],
    )
    low = move(normed, UP)
    far = move(normed, ACROSS)
    high = move(normed, DOWN)
    low, _ = lax.optimization_barrier((low, aside))
    near = call(stack_body, [("vmem", (288, 2048), BF16)], tag("vmem", normed, low, high))
    blocks = [normed, low, high, far, move(near, SWAP), move(far, SWAP)]

    w_sent = w_out
    w_up = move(w_sent, UP)
    w_down = move(w_sent, DOWN)

    payload, kqv, level, rows = call(
        state_body,
        [
            ("vmem", (8, PAYLOAD, 128), BF16),
            ("hbm", (768, 256), BF16),
            ("hbm", (8, 128), F32),
            ("hbm", (768, 2048), BF16),
        ],
        tag("vmem", *blocks, *prepared, aside),
        [
            pltpu.VMEM((768, 2048), BF16),
            pltpu.VMEM((768, 256), BF16),
            pltpu.VMEM((8, 128), F32),
            pltpu.SemaphoreType.DMA((3,)),
        ],
    )
    received = to_all(payload, Y_GROUPS)
    local, tops = call(
        local_body,
        [("load", (768, 128), F32), ("load", (128, 128), F32)],
        tag("load", level, kqv),
        flops=10**9,
    )
    payload, before = call(
        line_body,
        [("vmem", (8, PAYLOAD, 128), BF16), ("load", (72, 128), F32)],
        tag("vmem", received) + tag("hbm", tops),
    )
    w_far = w_out
    w_far = move(w_far, ACROSS)
    received = to_all(payload, Z_GROUPS)
    out_gate, conv, edge = call(
        mixer_body,
        [("load", (768, 128), BF16), ("load", (768, 128), BF16), ("load", (32, 128), F32)],
        tag("hbm", rows, w_outer, w_inner, w_signal, w_gate)
        + tag("vmem", aside)
        + tag("hbm", before),
        [
            pltpu.VMEM((768, 2048), BF16),
            pltpu.VMEM((2048, 256), BF16),
            pltpu.VMEM((2048, 256), BF16),
            pltpu.SemaphoreType.DMA((5,)),
        ],
        flops=10**9,
    )
    both = call(
        final_body,
        [("vmem", (768, 256), BF16)],
        tag("vmem", received, aside)
        + tag("hbm", before, start_state, local, tops, out_gate, kqv, conv, edge),
        [
            pltpu.VMEM((72, 128), F32),
            pltpu.VMEM((64, 128), F32),
            pltpu.VMEM((128, 128), F32),
            pltpu.VMEM((768, 128), F32),
            pltpu.VMEM((768, 128), BF16),
            pltpu.VMEM((768, 128), BF16),
            pltpu.VMEM((768, 128), BF16),
            pltpu.VMEM((32, 128), F32),
            pltpu.SemaphoreType.DMA((8,)),
        ],
    )
    mixers = lax.all_to_all(both.reshape(4, 192, 256), "tp", 0, 0, axis_index_groups=X_GROUPS)
    sent, kept = call(
        project_body,
        [("vmem", (96, 2048), BF16), ("vmem", (96, 2048), F32)],
        tag("vmem", mixers) + tag("hbm", w_out) + tag("vmem", w_up, w_down) + tag("hbm", w_far),
        [pltpu.VMEM((512, 2048), BF16), pltpu.SemaphoreType.DMA((4, 2))],
    )
    other = move(sent, SWAP)
    return call(add_body, [("load", (96, 2048), BF16)], tag("vmem", kept, other))


def solution(mesh):
    in_specs = (
        P(("sp", "tp"), None),
        P(),
        P(None, "tp"),
        P(None, "tp"),
        P(None, "tp"),
        P(),
        P(None, "tp"),
        P(None, "tp"),
        P(None, "tp"),
        P(None, "tp"),
        P(),
        P(),
        P(),
        P(),
        P("sp"),
        P("sp", None),
        P(),
        P(),
        P(),
        P("tp", None),
        P("tp", None),
    )

    return jax.shard_map(
        on_device,
        mesh=mesh,
        in_specs=in_specs,
        out_specs=P(("sp", "tp"), None),
        check_vma=False,
    )
```

profile of v0, /device:TPU:1, one launch (start us, length us, event | category | flops | bytes accessed | tf_op | source)
XLA Modules:
  0.0 110.8 jit_solution(813169866501111024)
XLA Ops:
  0.0 1.2 %shard_map.199.normed.b0 = bf16[96,2048]{1,0:T(8,128)(2,1)S(1)} custom-call(bf16[96,2048]{1,0:T(8,128)(2,1)} %tokens.1, bf16[2048]{0:T(1024)(128)(2,1)} %gain.2), custom_call_target="tpu_custom_call" | custom-call | flops 100000000 | bytes 1048576 | tf_op jit(solution)/shard_map/pallas_call | solution.py:28
  1.2 3.9 %collective-permute-start = (bf16[96,2048]{1,0:T(8,128)(2,1)S(1)}, bf16[96,2048]{1,0:T(8,128)(2,1)S(1)}, u32[]{:S(2)}, u32[]{:S(2)}) collective-permute-start(bf16[96,2048]{1,0:T(8,128)(2,1)S(1)} %shard_map.199.normed.b0), channel_id=1, source_target_pairs={{0,2},{1,3},{2,4},{3,5},{4,6},{5,7},{6,0},{7,1},{8,10},{9,11},{10,... | collective-permute-start | bytes 1179656 | tf_op jit(solution)/shard_map/ppermute | solution.py:422
  5.1 3.2 %collective-permute-start.1 = (bf16[96,2048]{1,0:T(8,128)(2,1)S(1)}, bf16[96,2048]{1,0:T(8,128)(2,1)S(1)}, u32[]{:S(2)}, u32[]{:S(2)}) collective-permute-start(bf16[96,2048]{1,0:T(8,128)(2,1)S(1)} %shard_map.199.normed.b0), channel_id=1, source_target_pairs={{0,6},{1,7},{2,0},{3,1},{4,2},{5,3},{6,4},{7,5},{8,14},{9,15},{10,... | collective-permute-start | bytes 1179656 | tf_op jit(solution)/shard_map/ppermute | solution.py:422
  8.3 2.8 %shard_map.200 = (bf16[256,2048]{1,0:T(8,128)(2,1)S(1)}, bf16[2048,128]{1,0:T(8,128)(2,1)S(1)}, bf16[2048,256]{1,0:T(8,128)(2,1)S(1)}, bf16[256,2048]{1,0:T(8,128)(2,1)S(1)}, f32[48,128]{1,0:T(8,128)S(1)}) custom-call(f32[8]{0:T(128)} %in_bias.1, f32[8]{0:T(128)} %forget_bias.1, f32[8]{0:T(128)} %start_scale.1, bf16[96,2048]{1,0:T(8,128)(2,1)S(1)} %shard_map.199.normed.b0, ...), custom_call_target="tpu_custom_call" | custom-call | flops 100000000 | bytes 1048576 | tf_op jit(solution)/shard_map/pallas_call | solution.py:28
  11.1 0.0 copy-start
  11.1 0.4 collective-permute-done.b1
  11.6 2.1 %collective-permute-done.1.b2 = bf16[96,2048]{1,0:T(8,128)(2,1)S(1)} collective-permute-done((bf16[96,2048]{1,0:T(8,128)(2,1)S(1)}, bf16[96,2048]{1,0:T(8,128)(2,1)S(1)}, u32[]{:S(2)}, u32[]{:S(2)}) %collective-permute-start.1) | collective-permute-done | bytes 393248 | tf_op jit(solution)/shard_map/ppermute | solution.py:422
  13.7 0.1 shard_map.201
  13.7 8.6 %collective-permute-start.3 = (bf16[288,2048]{1,0:T(8,128)(2,1)S(1)}, bf16[288,2048]{1,0:T(8,128)(2,1)S(1)}, u32[]{:S(2)}, u32[]{:S(2)}) collective-permute-start(bf16[288,2048]{1,0:T(8,128)(2,1)S(1)} %shard_map.201), channel_id=1, source_target_pairs={{0,1},{1,0},{2,3},{3,2},{4,5},{5,4},{6,7},{7,6},{8,9},{9,8},{10,11... | collective-permute-start | bytes 3538952 | tf_op jit(solution)/shard_map/ppermute | solution.py:422
  22.4 3.6 %collective-permute-start.2 = (bf16[96,2048]{1,0:T(8,128)(2,1)S(1)}, bf16[96,2048]{1,0:T(8,128)(2,1)S(1)}, u32[]{:S(2)}, u32[]{:S(2)}) collective-permute-start(bf16[96,2048]{1,0:T(8,128)(2,1)S(1)} %shard_map.199.normed.b0), channel_id=1, source_target_pairs={{0,4},{1,5},{2,6},{3,7},{4,0},{5,1},{6,2},{7,3},{8,12},{9,13},{10,... | collective-permute-start | bytes 1179656 | tf_op jit(solution)/shard_map/ppermute | solution.py:422
  25.9 10.5 %collective-permute-done.2.b3 = bf16[96,2048]{1,0:T(8,128)(2,1)S(1)} collective-permute-done((bf16[96,2048]{1,0:T(8,128)(2,1)S(1)}, bf16[96,2048]{1,0:T(8,128)(2,1)S(1)}, u32[]{:S(2)}, u32[]{:S(2)}) %collective-permute-start.2) | collective-permute-done | bytes 393248 | tf_op jit(solution)/shard_map/ppermute | solution.py:422
  36.4 2.8 %collective-permute-start.4 = (bf16[96,2048]{1,0:T(8,128)(2,1)S(1)}, bf16[96,2048]{1,0:T(8,128)(2,1)S(1)}, u32[]{:S(2)}, u32[]{:S(2)}) collective-permute-start(bf16[96,2048]{1,0:T(8,128)(2,1)S(1)} %collective-permute-done.2.b3), channel_id=1, source_target_pairs={{0,1},{1,0},{2,3},{3,2},{4,5},{5,4},{6,7},{7,6},{8,9},{9,8},{10,11... | collective-permute-start | bytes 1179656 | tf_op jit(solution)/shard_map/ppermute | solution.py:422
  39.2 2.9 %collective-permute-start.5 = (bf16[256,2048]{1,0:T(8,128)(2,1)S(1)}, bf16[256,2048]{1,0:T(8,128)(2,1)S(1)}, u32[]{:S(2)}, u32[]{:S(2)}) collective-permute-start(bf16[256,2048]{1,0:T(8,128)(2,1)S(1)} %get-tuple-element.40.w0), channel_id=1, source_target_pairs={{0,2},{1,3},{2,4},{3,5},{4,6},{5,7},{6,0},{7,1},{8,10},{9,11},{10,... | collective-permute-start | bytes 3145736 | tf_op jit(solution)/shard_map/ppermute | solution.py:422
  42.1 4.3 %collective-permute-start.6 = (bf16[256,2048]{1,0:T(8,128)(2,1)S(1)}, bf16[256,2048]{1,0:T(8,128)(2,1)S(1)}, u32[]{:S(2)}, u32[]{:S(2)}) collective-permute-start(bf16[256,2048]{1,0:T(8,128)(2,1)S(1)} %get-tuple-element.40.w0), channel_id=1, source_target_pairs={{0,6},{1,7},{2,0},{3,1},{4,2},{5,3},{6,4},{7,5},{8,14},{9,15},{10,... | collective-permute-start | bytes 3145736 | tf_op jit(solution)/shard_map/ppermute | solution.py:422
  46.5 0.0 copy-done
  46.5 3.1 %collective-permute-start.7 = (bf16[256,2048]{1,0:T(8,128)(2,1)S(1)}, bf16[256,2048]{1,0:T(8,128)(2,1)}, u32[]{:S(2)}, u32[]{:S(2)}) collective-permute-start(bf16[256,2048]{1,0:T(8,128)(2,1)S(1)} %get-tuple-element.40.w0), channel_id=1, source_target_pairs={{0,4},{1,5},{2,6},{3,7},{4,0},{5,1},{6,2},{7,3},{8,12},{9,13},{10,... | collective-permute-start | bytes 3145736 | tf_op jit(solution)/shard_map/ppermute | solution.py:422
  49.6 0.0 collective-permute-done.4.b7
  49.6 0.0 collective-permute-done.3.twins
  49.6 5.4 %shard_map.202 = (bf16[8,80,128]{2,1,0:T(8,128)(2,1)}, bf16[768,256]{1,0:T(8,128)(2,1)}, f32[8,128]{1,0:T(8,128)}, bf16[768,2048]{1,0:T(8,128)(2,1)}) custom-call(bf16[96,2048]{1,0:T(8,128)(2,1)S(1)} %shard_map.199.normed.b0, bf16[96,2048]{1,0:T(8,128)(2,1)S(1)} %collective-permute-done.b1, bf16[96,2048]{1,0:T(8,128)(2,1)S(1)} %collective-permute-done.1.b2, ...), custom_call_target="tpu_custom_call" | custom-call | flops 100000000 | bytes 1048576 | tf_op jit(solution)/shard_map/pallas_call | solution.py:28
  54.9 4.3 %all-to-all-start = ((bf16[8,80,128]{2,1,0:T(8,128)(2,1)}), bf16[8,80,128]{2,1,0:T(8,128)(2,1)S(1)}, u32[]{:S(2)}, u32[]{:S(2)}) async-start(bf16[8,80,128]{2,1,0:T(8,128)(2,1)} %get-tuple-element.29), calls=%async_computation | async-start | bytes 327680 | tf_op jit(solution)/shard_map/all_to_all | solution.py:426
  59.3 3.5 %shard_map.203 = (f32[768,128]{1,0:T(8,128)}, f32[128,128]{1,0:T(8,128)}) custom-call(f32[8,128]{1,0:T(8,128)} %get-tuple-element.30.level_in, bf16[768,256]{1,0:T(8,128)(2,1)} %get-tuple-element.31.kqv.kqv_in), custom_call_target="tpu_custom_call" | custom-call | flops 1000000000 | bytes 1048576 | tf_op jit(solution)/shard_map/pallas_call | solution.py:28
  62.8 4.6 %all-to-all-done.received = bf16[8,80,128]{2,1,0:T(8,128)(2,1)S(1)} async-done(((bf16[8,80,128]{2,1,0:T(8,128)(2,1)}), bf16[8,80,128]{2,1,0:T(8,128)(2,1)S(1)}, u32[]{:S(2)}, u32[]{:S(2)}) %all-to-all-start) | async-done | bytes 163872 | tf_op jit(solution)/shard_map/all_to_all | solution.py:426
  67.3 0.8 shard_map.204
  68.1 10.0 %all-to-all-start.1 = ((bf16[8,80,128]{2,1,0:T(8,128)(2,1)}), bf16[8,80,128]{2,1,0:T(8,128)(2,1)S(1)}, u32[]{:S(2)}, u32[]{:S(2)}) async-start(bf16[8,80,128]{2,1,0:T(8,128)(2,1)} %get-tuple-element.33), calls=%async_computation.1 | async-start | bytes 327680 | tf_op jit(solution)/shard_map/all_to_all | solution.py:426
  78.1 6.6 %shard_map.205 = (bf16[768,128]{1,0:T(8,128)(2,1)}, bf16[768,128]{1,0:T(8,128)(2,1)}, f32[32,128]{1,0:T(8,128)}) custom-call(bf16[768,2048]{1,0:T(8,128)(2,1)} %get-tuple-element.36.rows_in, bf16[2048,128]{1,0:T(8,128)(2,1)} %w_outer.1, bf16[2048,128]{1,0:T(8,128)(2,1)} %w_inner.3, bf16[2048,128]{1,0:T(8,128)(2,1)} %w_signal.3, bf16[2048,128]{1,0:T(8,128)(2,1)} %w_gate.1, ...), custom_call_target="tpu_custom_call" | custom-call | flops 1000000000 | bytes 1048576 | tf_op jit(solution)/shard_map/pallas_call | solution.py:28
  84.7 1.7 %all-to-all-done.1.received = bf16[8,80,128]{2,1,0:T(8,128)(2,1)S(1)} async-done(((bf16[8,80,128]{2,1,0:T(8,128)(2,1)}), bf16[8,80,128]{2,1,0:T(8,128)(2,1)S(1)}, u32[]{:S(2)}, u32[]{:S(2)}) %all-to-all-start.1) | async-done | bytes 163872 | tf_op jit(solution)/shard_map/all_to_all | solution.py:426
  86.4 3.1 %shard_map.206 = bf16[768,256]{1,0:T(8,128)(2,1)} custom-call(bf16[8,80,128]{2,1,0:T(8,128)(2,1)S(1)} %all-to-all-done.1.received, f32[48,128]{1,0:T(8,128)S(1)} %get-tuple-element.24.aside, f32[72,128]{1,0:T(8,128)} %get-tuple-element.34.before.before_in, f32[8,64,128]{2,1,0:T(8,128)} %start_state.1, f32[768,128]{1,0:T(8,128)} %get-tuple-element.35.local_in, ...), custom_call_target="tpu_custom_call" | custom-call | flops 100000000 | bytes 1048576 | tf_op jit(solution)/shard_map/pallas_call | solution.py:28
  89.5 3.5 %all-to-all-start.2 = ((bf16[4,192,256]{2,1,0:T(8,128)(2,1)}), bf16[4,192,256]{2,1,0:T(8,128)(2,1)S(1)}, u32[]{:S(2)}, u32[]{:S(2)}) async-start(bf16[4,192,256]{2,1,0:T(8,128)(2,1)} %bitcast.5), calls=%async_computation.2 | async-start | bytes 786432 | tf_op jit(solution)/shard_map/all_to_all | solution.py:526
  93.0 0.0 collective-permute-done.5.w1
  93.0 0.0 collective-permute-done.6.w2
  93.0 0.0 collective-permute-done.7.w3
  93.1 6.2 %all-to-all-done.2.received = bf16[4,192,256]{2,1,0:T(8,128)(2,1)S(1)} async-done(((bf16[4,192,256]{2,1,0:T(8,128)(2,1)}), bf16[4,192,256]{2,1,0:T(8,128)(2,1)S(1)}, u32[]{:S(2)}, u32[]{:S(2)}) %all-to-all-start.2) | async-done | bytes 393248 | tf_op jit(solution)/shard_map/all_to_all | solution.py:526
  99.2 2.3 %shard_map.207 = (bf16[96,2048]{1,0:T(8,128)(2,1)S(1)}, f32[96,2048]{1,0:T(8,128)S(1)}) custom-call(bf16[4,192,256]{2,1,0:T(8,128)(2,1)S(1)} %all-to-all-done.2.received, bf16[256,2048]{1,0:T(8,128)(2,1)} %copy-done, bf16[256,2048]{1,0:T(8,128)(2,1)S(1)} %collective-permute-done.5.w1, bf16[256,2048]{1,0:T(8,128)(2,1)S(1)} %collective-permute-done.6.w2, ...), custom_call_target="tpu_custom_call" | custom-call | flops 100000000 | bytes 1048576 | tf_op jit(solution)/shard_map/pallas_call | solution.py:28
  101.5 7.1 %collective-permute-start.8 = (bf16[96,2048]{1,0:T(8,128)(2,1)S(1)}, bf16[96,2048]{1,0:T(8,128)(2,1)S(1)}, u32[]{:S(2)}, u32[]{:S(2)}) collective-permute-start(bf16[96,2048]{1,0:T(8,128)(2,1)S(1)} %get-tuple-element.42), channel_id=1, source_target_pairs={{0,1},{1,0},{2,3},{3,2},{4,5},{5,4},{6,7},{7,6},{8,9},{9,8},{10,11... | collective-permute-start | bytes 1179656 | tf_op jit(solution)/shard_map/ppermute | solution.py:422
  108.6 1.3 %collective-permute-done.8.other = bf16[96,2048]{1,0:T(8,128)(2,1)S(1)} collective-permute-done((bf16[96,2048]{1,0:T(8,128)(2,1)S(1)}, bf16[96,2048]{1,0:T(8,128)(2,1)S(1)}, u32[]{:S(2)}, u32[]{:S(2)}) %collective-permute-start.8) | collective-permute-done | bytes 393248 | tf_op jit(solution)/shard_map/ppermute | solution.py:422
  110.0 0.8 shard_map.208
Async XLA Ops:
  1.2 10.4 %collective-permute-start = (bf16[96,2048]{1,0:T(8,128)(2,1)S(1)}, bf16[96,2048]{1,0:T(8,128)(2,1)S(1)}, u32[]{:S(2)}, u32[]{:S(2)}) collective-permute-start(bf16[96,2048]{1,0:T(8,128)(2,1)S(1)} %shard_map.199.normed.b0), channel_id=1, source_target_pairs={{0,2},{1,3},{2,4},{3,5},{4,6},{5,7},{6,0},{7,1},{8,10},{9,11},{10,... | collective-permute-start | bytes 1179656 | tf_op jit(solution)/shard_map/ppermute | solution.py:422
  5.1 8.5 %collective-permute-start.1 = (bf16[96,2048]{1,0:T(8,128)(2,1)S(1)}, bf16[96,2048]{1,0:T(8,128)(2,1)S(1)}, u32[]{:S(2)}, u32[]{:S(2)}) collective-permute-start(bf16[96,2048]{1,0:T(8,128)(2,1)S(1)} %shard_map.199.normed.b0), channel_id=1, source_target_pairs={{0,6},{1,7},{2,0},{3,1},{4,2},{5,3},{6,4},{7,5},{8,14},{9,15},{10,... | collective-permute-start | bytes 1179656 | tf_op jit(solution)/shard_map/ppermute | solution.py:422
  11.1 35.3 %copy-start = (bf16[256,2048]{1,0:T(8,128)(2,1)}, bf16[256,2048]{1,0:T(8,128)(2,1)S(1)}, u32[]{:S(2)}) copy-start(bf16[256,2048]{1,0:T(8,128)(2,1)S(1)} %get-tuple-element.40.w0) | copy-start | bytes 3145732
  13.7 35.8 %collective-permute-start.3 = (bf16[288,2048]{1,0:T(8,128)(2,1)S(1)}, bf16[288,2048]{1,0:T(8,128)(2,1)S(1)}, u32[]{:S(2)}, u32[]{:S(2)}) collective-permute-start(bf16[288,2048]{1,0:T(8,128)(2,1)S(1)} %shard_map.201), channel_id=1, source_target_pairs={{0,1},{1,0},{2,3},{3,2},{4,5},{5,4},{6,7},{7,6},{8,9},{9,8},{10,11... | collective-permute-start | bytes 3538952 | tf_op jit(solution)/shard_map/ppermute | solution.py:422
  22.4 14.1 %collective-permute-start.2 = (bf16[96,2048]{1,0:T(8,128)(2,1)S(1)}, bf16[96,2048]{1,0:T(8,128)(2,1)S(1)}, u32[]{:S(2)}, u32[]{:S(2)}) collective-permute-start(bf16[96,2048]{1,0:T(8,128)(2,1)S(1)} %shard_map.199.normed.b0), channel_id=1, source_target_pairs={{0,4},{1,5},{2,6},{3,7},{4,0},{5,1},{6,2},{7,3},{8,12},{9,13},{10,... | collective-permute-start | bytes 1179656 | tf_op jit(solution)/shard_map/ppermute | solution.py:422
  36.4 13.1 %collective-permute-start.4 = (bf16[96,2048]{1,0:T(8,128)(2,1)S(1)}, bf16[96,2048]{1,0:T(8,128)(2,1)S(1)}, u32[]{:S(2)}, u32[]{:S(2)}) collective-permute-start(bf16[96,2048]{1,0:T(8,128)(2,1)S(1)} %collective-permute-done.2.b3), channel_id=1, source_target_pairs={{0,1},{1,0},{2,3},{3,2},{4,5},{5,4},{6,7},{7,6},{8,9},{9,8},{10,11... | collective-permute-start | bytes 1179656 | tf_op jit(solution)/shard_map/ppermute | solution.py:422
  39.2 53.8 %collective-permute-start.5 = (bf16[256,2048]{1,0:T(8,128)(2,1)S(1)}, bf16[256,2048]{1,0:T(8,128)(2,1)S(1)}, u32[]{:S(2)}, u32[]{:S(2)}) collective-permute-start(bf16[256,2048]{1,0:T(8,128)(2,1)S(1)} %get-tuple-element.40.w0), channel_id=1, source_target_pairs={{0,2},{1,3},{2,4},{3,5},{4,6},{5,7},{6,0},{7,1},{8,10},{9,11},{10,... | collective-permute-start | bytes 3145736 | tf_op jit(solution)/shard_map/ppermute | solution.py:422
  42.1 50.9 %collective-permute-start.6 = (bf16[256,2048]{1,0:T(8,128)(2,1)S(1)}, bf16[256,2048]{1,0:T(8,128)(2,1)S(1)}, u32[]{:S(2)}, u32[]{:S(2)}) collective-permute-start(bf16[256,2048]{1,0:T(8,128)(2,1)S(1)} %get-tuple-element.40.w0), channel_id=1, source_target_pairs={{0,6},{1,7},{2,0},{3,1},{4,2},{5,3},{6,4},{7,5},{8,14},{9,15},{10,... | collective-permute-start | bytes 3145736 | tf_op jit(solution)/shard_map/ppermute | solution.py:422
  46.5 46.6 %collective-permute-start.7 = (bf16[256,2048]{1,0:T(8,128)(2,1)S(1)}, bf16[256,2048]{1,0:T(8,128)(2,1)}, u32[]{:S(2)}, u32[]{:S(2)}) collective-permute-start(bf16[256,2048]{1,0:T(8,128)(2,1)S(1)} %get-tuple-element.40.w0), channel_id=1, source_target_pairs={{0,4},{1,5},{2,6},{3,7},{4,0},{5,1},{6,2},{7,3},{8,12},{9,13},{10,... | collective-permute-start | bytes 3145736 | tf_op jit(solution)/shard_map/ppermute | solution.py:422
  54.9 12.4 %all-to-all-start = ((bf16[8,80,128]{2,1,0:T(8,128)(2,1)}), bf16[8,80,128]{2,1,0:T(8,128)(2,1)S(1)}, u32[]{:S(2)}, u32[]{:S(2)}) async-start(bf16[8,80,128]{2,1,0:T(8,128)(2,1)} %get-tuple-element.29), calls=%async_computation | async-start | bytes 327680 | tf_op jit(solution)/shard_map/all_to_all | solution.py:426
  68.1 18.3 %all-to-all-start.1 = ((bf16[8,80,128]{2,1,0:T(8,128)(2,1)}), bf16[8,80,128]{2,1,0:T(8,128)(2,1)S(1)}, u32[]{:S(2)}, u32[]{:S(2)}) async-start(bf16[8,80,128]{2,1,0:T(8,128)(2,1)} %get-tuple-element.33), calls=%async_computation.1 | async-start | bytes 327680 | tf_op jit(solution)/shard_map/all_to_all | solution.py:426
  89.5 9.7 %all-to-all-start.2 = ((bf16[4,192,256]{2,1,0:T(8,128)(2,1)}), bf16[4,192,256]{2,1,0:T(8,128)(2,1)S(1)}, u32[]{:S(2)}, u32[]{:S(2)}) async-start(bf16[4,192,256]{2,1,0:T(8,128)(2,1)} %bitcast.5), calls=%async_computation.2 | async-start | bytes 786432 | tf_op jit(solution)/shard_map/all_to_all | solution.py:526
  101.5 8.5 %collective-permute-start.8 = (bf16[96,2048]{1,0:T(8,128)(2,1)S(1)}, bf16[96,2048]{1,0:T(8,128)(2,1)S(1)}, u32[]{:S(2)}, u32[]{:S(2)}) collective-permute-start(bf16[96,2048]{1,0:T(8,128)(2,1)S(1)} %get-tuple-element.42), channel_id=1, source_target_pairs={{0,1},{1,0},{2,3},{3,2},{4,5},{5,4},{6,7},{7,6},{8,9},{9,8},{10,11... | collective-permute-start | bytes 1179656 | tf_op jit(solution)/shard_map/ppermute | solution.py:422
where the time goes:
time: 112 us; the launch traced here: 111 us
  starting transfers between devices  57.4 us (51%)
  waiting for transfers between devices  26.8 us (24%)
  Pallas kernels  26.4 us (24%)
    ppermute x9, starting transfers between devices, move(): return lax.ppermute(value, 'tp', pairs)  39.5 us
    pallas_call x10, Pallas kernels, call(): pl.pallas_call(body, out_shape=tuple((SPACES[how][0](shape, kind) for how...  26.4 us
    all_to_all x2, starting transfers between devices, to_all(): return lax.all_to_all(copies, 'sp', 0, 0, axis_index_groups=groups)  14.4 us
    ppermute x9, waiting for transfers between devices, move(): return lax.ppermute(value, 'tp', pairs)  14.3 us
    all_to_all x2, waiting for transfers between devices, to_all(): return lax.all_to_all(copies, 'sp', 0, 0, axis_index_groups=groups)  6.27 us
    all_to_all x1, waiting for transfers between devices, on_device(): lax.all_to_all(both.reshape(4, 192, 256), 'tp', 0, 0, axis_index_groups=X...  6.16 us
    all_to_all x1, starting transfers between devices, on_device(): lax.all_to_all(both.reshape(4, 192, 256), 'tp', 0, 0, axis_index_groups=X...  3.47 us
  transfers between devices with their start and end apart: 12, of which 7 were waited for; matrix products, arithmetic and copies ran while one was open for 0% of the time, Pallas kernels for 20%

commit v1 on v0

--- a/solution.py
+++ b/solution.py
@@ -14,7 +14,7 @@
 FLOOR = -1e30
 F32 = jnp.float32
 BF16 = jnp.bfloat16
-PAYLOAD = 80
+PAYLOAD = 72
 
 SPACES = {
     "vmem": (pltpu.VMEM, pltpu.VMEM),
@@ -79,6 +79,15 @@
     rest = value - high
     middle = rest.astype(BF16).astype(F32)
     return [high, middle, rest - middle]
+
+
+def packed(state, peak, decay, rim):
+    lane = lax.broadcasted_iota(jnp.int32, (1, 128), 1)
+    scales = jnp.zeros((1, 128), F32)
+    for i, term in enumerate(split3(peak) + split3(decay)):
+        scales = jnp.where(lane == i, term, scales)
+    rows = [state, scales, rim, jnp.zeros((PAYLOAD - 69, 128), F32)]
+    return jnp.concatenate(rows, axis=0).astype(BF16)
 
 
 def lane_scan(value, op, neutral):
@@ -157,6 +166,8 @@
     ]
     savings[0].start()
     first = dot(rows[...], w_turned[...], ((1,), (1,)))
+    values = dot(rows[...], w_value[...]).astype(BF16)
+    rim = dot(rows[752:768, :], w_rim[...])
     turned = [jnp.transpose(first[128 * b : 128 * (b + 1), 128:256]) for b in range(6)]
     mine = lax.broadcasted_iota(jnp.int32, (8, 128), 0) == head
     pick = lambda part: jnp.sum(jnp.where(mine, part, 0.0), axis=0, keepdims=True)
@@ -182,7 +193,6 @@
     peak = jnp.broadcast_to(total + highest, (1, 128))
     weight = jnp.exp(level - highest)
     columns = jnp.transpose(jnp.concatenate([weight, jnp.zeros((120, 128), F32)], axis=0))
-    values = dot(rows[...], w_value[...]).astype(BF16)
     kqv[:, 0:128] = first[:, 0:128].astype(BF16)
     kqv[:, 128:256] = values
     savings[1].start()
@@ -193,16 +203,10 @@
         keys = first[128 * b : 128 * (b + 1), 0:DQK].astype(BF16).astype(F32)
         pieces.append((keys * columns[:, b : b + 1]).astype(BF16))
     state = dot(jnp.concatenate(pieces, axis=0), values, ((0,), (0,)))
-    rim = dot(rows[752:768, :], w_rim[...])
-    packed = jnp.concatenate(
-        [state]
-        + split3(peak)
-        + split3(jnp.broadcast_to(total, (1, 128)))
-        + [rim[14:16, 0:128], rim[14:16, 128:256], jnp.zeros((PAYLOAD - 74, 128), F32)],
-        axis=0,
-    ).astype(BF16)
+    rims = jnp.concatenate([rim[14:16, 0:128], rim[14:16, 128:256]], axis=0)
+    sent = packed(state, peak, jnp.broadcast_to(total, (1, 128)), rims)
     for i in range(8):
-        payload[i] = packed
+        payload[i] = sent
     for saving in savings:
         saving.wait()
 
@@ -227,30 +231,34 @@
                 power = jnp.where(causal, power, FLOOR)
             parts.append((scores[:, 128 * u : 128 * (u + 1)] * jnp.exp(power)).astype(BF16))
         weights = parts[0] if b == 0 else jnp.concatenate(parts, axis=1)
-        local_out[128 * b : high, :] = dot(weights, kqv[0:high, 128:256])
+        local_out[128 * b : high, :] = dot(weights, kqv[0:high, 128:256]).astype(BF16)
 
 
 def mixer_body(
-    rows_in, w_outer, w_inner, w_signal, w_gate, aside, before,
-    gate_out, conv_out, edge_out, rows, w_one, w_two, sems,
+    rows_in, w_outer, w_inner, w_signal, w_gate, aside, before_in, start_state, local_in, tops_in,
+    kqv_in, gate_out, conv_out, edge_out, before, first_state, tops, local, query,
+    rows, w_all, sems,
 ):
     loads = [
-        pltpu.make_async_copy(w_outer, w_one.at[:, 0:128], sems.at[0]),
-        pltpu.make_async_copy(w_inner, w_one.at[:, 128:256], sems.at[1]),
+        pltpu.make_async_copy(w_outer, w_all.at[:, 0:128], sems.at[0]),
+        pltpu.make_async_copy(w_inner, w_all.at[:, 128:256], sems.at[1]),
         pltpu.make_async_copy(rows_in, rows, sems.at[2]),
-        pltpu.make_async_copy(w_signal, w_two.at[:, 0:128], sems.at[3]),
-        pltpu.make_async_copy(w_gate, w_two.at[:, 128:256], sems.at[4]),
+        pltpu.make_async_copy(w_signal, w_all.at[:, 256:384], sems.at[3]),
+        pltpu.make_async_copy(w_gate, w_all.at[:, 384:512], sems.at[4]),
+        pltpu.make_async_copy(before_in, before, sems.at[5]),
+        pltpu.make_async_copy(start_state.at[own_tp()], first_state, sems.at[6]),
+        pltpu.make_async_copy(tops_in, tops, sems.at[7]),
+        pltpu.make_async_copy(local_in, local, sems.at[8]),
+        pltpu.make_async_copy(kqv_in.at[:, 0:128], query, sems.at[9]),
     ]
     for load in loads:
         load.start()
-    for load in loads[0:3]:
+    for load in loads[0:5]:
         load.wait()
-    first = dot(rows[...], w_one[...])
+    first = dot(rows[...], w_all[:, 0:256])
+    second = dot(rows[...], w_all[:, 256:512])
     outer = first[:, 0:128].astype(BF16).astype(F32)
     inner = first[:, 128:256].astype(BF16).astype(F32)
-    for load in loads[3:5]:
-        load.wait()
-    second = dot(rows[...], w_two[...])
     signal = second[:, 0:128].astype(BF16).astype(F32)
     gate_out[...] = jax.nn.sigmoid(second[:, 128:256].astype(BF16).astype(F32)).astype(BF16)
     tap = aside[40:43, :]
@@ -262,6 +270,8 @@
     conv_out[...] = (outer * summed).astype(BF16)
     edge_out[0:16, :] = summed[0:16]
     edge_out[16:32, :] = outer[0:16]
+    for load in loads[5:]:
+        load.wait()
 
 
 def merged(states, peaks, decays, allowed, upto):
@@ -280,12 +290,16 @@
 
 
 def unpack(received):
-    wide = [received[i].astype(F32) for i in range(8)]
+    wide = [received[(i + 4) % 8].astype(F32) for i in range(8)]
+    scales = jnp.concatenate([w[64:65] for w in wide], axis=0)
+    scales = scales + pltpu.roll(scales, 127, 1) + pltpu.roll(scales, 126, 1)
+    peaks = jnp.broadcast_to(scales[:, 0:1], (8, 128))
+    decays = jnp.broadcast_to(scales[:, 3:4], (8, 128))
     return (
         [w[0:64] for w in wide],
-        [w[64:65] + w[65:66] + w[66:67] for w in wide],
-        [w[67:68] + w[68:69] + w[69:70] for w in wide],
-        [w[70:74] for w in wide],
+        [peaks[i : i + 1] for i in range(8)],
+        [decays[i : i + 1] for i in range(8)],
+        [w[65:69] for w in wide],
     )
 
 
@@ -294,12 +308,9 @@
     states, peaks, decays, rims = unpack(received)
     every = [True] * 8
     state, peak, decay = merged(states, peaks, decays, every, every)
-    packed = jnp.concatenate(
-        [state] + split3(peak) + split3(decay) + [rims[7], jnp.zeros((PAYLOAD - 74, 128), F32)],
-        axis=0,
-    ).astype(BF16)
+    sent = packed(state, peak, decay, rims[7])
     for i in range(8):
-        payload[i] = packed
+        payload[i] = sent
     earlier = [i < me for i in range(8)]
     state, peak, decay = merged(states, peaks, decays, earlier, earlier)
     rim = jnp.zeros((4, 128), F32)
@@ -310,48 +321,29 @@
 
 
 def final_body(
-    received, aside, before_in, start_state, local_in, tops_in, gate_in, kqv_in, conv_in, edge_in,
-    out, before, first_state, tops, local, out_gate, kqv, conv, edge, sems,
+    received, aside, out_gate, conv, edge, before, first_state, tops, local, kqv, out
 ):
-    head, y, z = own_tp(), own_sp() % 8, own_sp() // 8
-    loads = [
-        (start_state.at[head], first_state),
-        (before_in, before),
-        (tops_in, tops),
-        (kqv_in.at[:, 0:128], kqv),
-        (local_in, local),
-        (gate_in, out_gate),
-        (conv_in, conv),
-        (edge_in, edge),
-    ]
-    loads = [pltpu.make_async_copy(a, b, sems.at[i]) for i, (a, b) in enumerate(loads)]
-    for load in loads:
-        load.start()
+    y, z = own_sp() % 8, own_sp() // 8
     states, peaks, decays, rims = unpack(received)
     earlier = [i < z for i in range(8)]
     state, peak, decay = merged(states, peaks, decays, earlier, earlier)
     lifted = aside[32:33, :] + decay
     ceiling = jnp.maximum(lifted, peak)
-    loads[0].wait()
     state = jnp.exp(lifted - ceiling) * first_state[...] + jnp.exp(peak - ceiling) * state
-    loads[1].wait()
     lifted = ceiling + before[65:66, :]
     peak = before[64:65, :]
     ceiling = jnp.maximum(lifted, peak)
     state = jnp.exp(lifted - ceiling) * state + jnp.exp(peak - ceiling) * before[0:64, :]
     state = (state * DQK**-0.5).astype(BF16)
-    loads[2].wait()
     top = tops[...]
     best = jnp.maximum(top, ceiling)
     keep = jnp.exp(top - best)
     bring = jnp.exp(ceiling - best)
-    for load in loads[3:]:
-        load.wait()
     scale = aside[43:44, :]
     for b in range(6):
         here = slice(128 * b, 128 * (b + 1))
         remote = dot(kqv[here, DQK : 2 * DQK], state)
-        number = bring[:, b : b + 1] * remote + keep[:, b : b + 1] * local[here, :]
+        number = bring[:, b : b + 1] * remote + keep[:, b : b + 1] * local[here, :].astype(F32)
         spread = lax.rsqrt(jnp.mean(number * number, axis=1, keepdims=True) + EPS)
         out[here, 128:256] = (number * spread * scale * out_gate[here, :].astype(F32)).astype(BF16)
     out[:, 0:128] = conv[...]
@@ -372,7 +364,7 @@
     x, core = tp // 2, tp % 2
     loads = []
     for n in range(4):
-        for i, weight in enumerate((w0, w3)):
+        for i, weight in enumerate((w0, w2, w3)):
             cut = pl.ds(512 * n, 512)
             loads.append(
                 pltpu.make_async_copy(
@@ -383,16 +375,19 @@
         load.start()
     there = pl.ds(pl.multiple_of((1 - core) * 96, 32), 96)
     here = pl.ds(pl.multiple_of(core * 96, 32), 96)
-    parts = [
-        jnp.concatenate([received[(x + shift) % 4, rows, :] for rows in (there, here)], axis=0)
-        for shift in (0, 3, 1, 2)
-    ]
+    both = jnp.concatenate(
+        [
+            jnp.concatenate([received[(x + shift) % 4, rows, :] for shift in (0, 1, 2)], axis=1)
+            for rows in (there, here)
+        ],
+        axis=0,
+    )
+    low = jnp.concatenate([received[(x + 3) % 4, rows, :] for rows in (there, here)], axis=0)
     for n in range(4):
+        for load in loads[3 * n : 3 * n + 3]:
+            load.wait()
         cut = slice(512 * n, 512 * (n + 1))
-        total = dot(parts[1], w1[:, cut]) + dot(parts[2], w2[:, cut])
-        for load in loads[2 * n : 2 * n + 2]:
-            load.wait()
-        total = total + dot(parts[0], weights[0:256, cut]) + dot(parts[3], weights[256:512, cut])
+        total = dot(low, w1[:, cut]) + dot(both, weights[:, cut])
         sent[:, cut] = total[0:96].astype(BF16)
         kept[:, cut] = total[96:192]
 
@@ -414,8 +409,9 @@
 ACROSS = tp_moves(lambda x, c: (x + 2, c))
 SWAP = tp_moves(lambda x, c: (x, 1 - c))
 X_GROUPS = [[0, 2, 4, 6], [1, 3, 5, 7]]
-Y_GROUPS = [[z * 8 + y for y in range(8)] for z in range(8)]
-Z_GROUPS = [[z * 8 + y for z in range(8)] for y in range(8)]
+TURN = (4, 5, 6, 7, 0, 1, 2, 3)
+Y_GROUPS = [[z * 8 + y for y in TURN] for z in range(8)]
+Z_GROUPS = [[z * 8 + y for z in TURN] for y in range(8)]
 
 
 def move(value, pairs):
@@ -480,7 +476,7 @@
     received = to_all(payload, Y_GROUPS)
     local, tops = call(
         local_body,
-        [("load", (768, 128), F32), ("load", (128, 128), F32)],
+        [("load", (768, 128), BF16), ("load", (128, 128), F32)],
         tag("load", level, kqv),
         flops=10**9,
     )
@@ -492,43 +488,37 @@
     w_far = w_out
     w_far = move(w_far, ACROSS)
     received = to_all(payload, Z_GROUPS)
-    out_gate, conv, edge = call(
+    prefetched = call(
         mixer_body,
-        [("load", (768, 128), BF16), ("load", (768, 128), BF16), ("load", (32, 128), F32)],
+        [
+            ("vmem", (768, 128), BF16),
+            ("vmem", (768, 128), BF16),
+            ("vmem", (32, 128), F32),
+            ("vmem", (72, 128), F32),
+            ("vmem", (64, 128), F32),
+            ("vmem", (128, 128), F32),
+            ("vmem", (768, 128), BF16),
+            ("vmem", (768, 128), BF16),
+        ],
         tag("hbm", rows, w_outer, w_inner, w_signal, w_gate)
         + tag("vmem", aside)
-        + tag("hbm", before),
+        + tag("hbm", before, start_state, local, tops, kqv),
         [
             pltpu.VMEM((768, 2048), BF16),
-            pltpu.VMEM((2048, 256), BF16),
-            pltpu.VMEM((2048, 256), BF16),
-            pltpu.SemaphoreType.DMA((5,)),
+            pltpu.VMEM((2048, 512), BF16),
+            pltpu.SemaphoreType.DMA((10,)),
         ],
         flops=10**9,
     )
     both = call(
-        final_body,
-        [("vmem", (768, 256), BF16)],
-        tag("vmem", received, aside)
-        + tag("hbm", before, start_state, local, tops, out_gate, kqv, conv, edge),
-        [
-            pltpu.VMEM((72, 128), F32),
-            pltpu.VMEM((64, 128), F32),
-            pltpu.VMEM((128, 128), F32),
-            pltpu.VMEM((768, 128), F32),
-            pltpu.VMEM((768, 128), BF16),
-            pltpu.VMEM((768, 128), BF16),
-            pltpu.VMEM((768, 128), BF16),
-            pltpu.VMEM((32, 128), F32),
-            pltpu.SemaphoreType.DMA((8,)),
-        ],
+        final_body, [("vmem", (768, 256), BF16)], tag("vmem", received, aside, *prefetched)
     )
     mixers = lax.all_to_all(both.reshape(4, 192, 256), "tp", 0, 0, axis_index_groups=X_GROUPS)
     sent, kept = call(
         project_body,
         [("vmem", (96, 2048), BF16), ("vmem", (96, 2048), F32)],
-        tag("vmem", mixers) + tag("hbm", w_out) + tag("vmem", w_up, w_down) + tag("hbm", w_far),
-        [pltpu.VMEM((512, 2048), BF16), pltpu.SemaphoreType.DMA((4, 2))],
+        tag("vmem", mixers) + tag("hbm", w_out) + tag("vmem", w_up) + tag("hbm", w_down, w_far),
+        [pltpu.VMEM((768, 2048), BF16), pltpu.SemaphoreType.DMA((4, 3))],
     )
     other = move(sent, SWAP)
     return call(add_body, [("load", (96, 2048), BF16)], tag("vmem", kept, other))

time: 112 us -> 105 us (0.938)
  the two profiles are of different devices: /device:TPU:1 before, /device:TPU:3 now
where the time goes in v1:
time: 105 us; the launch traced here: 104 us
  starting transfers between devices  54.8 us (52%)
  waiting for transfers between devices  27.4 us (26%)
  Pallas kernels  21.7 us (21%)
    ppermute x9, starting transfers between devices, move(): return lax.ppermute(value, 'tp', pairs)  31.2 us
    ppermute x9, waiting for transfers between devices, move(): return lax.ppermute(value, 'tp', pairs)  23.3 us
    pallas_call x10, Pallas kernels, call(): pl.pallas_call(body, out_shape=tuple((SPACES[how][0](shape, kind) for how...  21.7 us
    all_to_all x2, starting transfers between devices, to_all(): return lax.all_to_all(copies, 'sp', 0, 0, axis_index_groups=groups)  19.4 us
    all_to_all x1, starting transfers between devices, on_device(): lax.all_to_all(both.reshape(4, 192, 256), 'tp', 0, 0, axis_index_groups=X...  4.22 us
    all_to_all x1, waiting for transfers between devices, on_device(): lax.all_to_all(both.reshape(4, 192, 256), 'tp', 0, 0, axis_index_groups=X...  4.11 us
  transfers between devices with their start and end apart: 12, of which 6 were waited for; matrix products, arithmetic and copies ran while one was open for 0% of the time, Pallas kernels for 16%

profile of v1, /device:TPU:3, one launch (start us, length us, event | category | flops | bytes accessed | tf_op | source)
XLA Modules:
  0.0 104.1 jit_solution(18355825123289452912)
XLA Ops:
  0.0 1.2 %shard_map.199.normed.b0 = bf16[96,2048]{1,0:T(8,128)(2,1)S(1)} custom-call(bf16[96,2048]{1,0:T(8,128)(2,1)} %tokens.1, bf16[2048]{0:T(1024)(128)(2,1)} %gain.2), custom_call_target="tpu_custom_call" | custom-call | flops 100000000 | bytes 1048576 | tf_op jit(solution)/shard_map/pallas_call | solution.py:28
  1.2 3.1 %collective-permute-start = (bf16[96,2048]{1,0:T(8,128)(2,1)S(1)}, bf16[96,2048]{1,0:T(8,128)(2,1)S(1)}, u32[]{:S(2)}, u32[]{:S(2)}) collective-permute-start(bf16[96,2048]{1,0:T(8,128)(2,1)S(1)} %shard_map.199.normed.b0), channel_id=1, source_target_pairs={{0,2},{1,3},{2,4},{3,5},{4,6},{5,7},{6,0},{7,1},{8,10},{9,11},{10,... | collective-permute-start | bytes 1179656 | tf_op jit(solution)/shard_map/ppermute | solution.py:418
  4.3 2.2 %collective-permute-start.1 = (bf16[96,2048]{1,0:T(8,128)(2,1)S(1)}, bf16[96,2048]{1,0:T(8,128)(2,1)S(1)}, u32[]{:S(2)}, u32[]{:S(2)}) collective-permute-start(bf16[96,2048]{1,0:T(8,128)(2,1)S(1)} %shard_map.199.normed.b0), channel_id=1, source_target_pairs={{0,6},{1,7},{2,0},{3,1},{4,2},{5,3},{6,4},{7,5},{8,14},{9,15},{10,... | collective-permute-start | bytes 1179656 | tf_op jit(solution)/shard_map/ppermute | solution.py:418
  6.5 2.8 %shard_map.200 = (bf16[256,2048]{1,0:T(8,128)(2,1)S(1)}, bf16[2048,128]{1,0:T(8,128)(2,1)S(1)}, bf16[2048,256]{1,0:T(8,128)(2,1)S(1)}, bf16[256,2048]{1,0:T(8,128)(2,1)S(1)}, f32[48,128]{1,0:T(8,128)S(1)}) custom-call(f32[8]{0:T(128)} %in_bias.1, f32[8]{0:T(128)} %forget_bias.1, f32[8]{0:T(128)} %start_scale.1, bf16[96,2048]{1,0:T(8,128)(2,1)S(1)} %shard_map.199.normed.b0, ...), custom_call_target="tpu_custom_call" | custom-call | flops 100000000 | bytes 1048576 | tf_op jit(solution)/shard_map/pallas_call | solution.py:28
  9.3 0.0 copy-start
  9.3 2.8 %collective-permute-done.b1 = bf16[96,2048]{1,0:T(8,128)(2,1)S(1)} collective-permute-done((bf16[96,2048]{1,0:T(8,128)(2,1)S(1)}, bf16[96,2048]{1,0:T(8,128)(2,1)S(1)}, u32[]{:S(2)}, u32[]{:S(2)}) %collective-permute-start) | collective-permute-done | bytes 393248 | tf_op jit(solution)/shard_map/ppermute | solution.py:418
  12.1 3.8 %collective-permute-done.1.b2 = bf16[96,2048]{1,0:T(8,128)(2,1)S(1)} collective-permute-done((bf16[96,2048]{1,0:T(8,128)(2,1)S(1)}, bf16[96,2048]{1,0:T(8,128)(2,1)S(1)}, u32[]{:S(2)}, u32[]{:S(2)}) %collective-permute-start.1) | collective-permute-done | bytes 393248 | tf_op jit(solution)/shard_map/ppermute | solution.py:418
  15.9 0.1 shard_map.201
  16.0 3.7 %collective-permute-start.3 = (bf16[288,2048]{1,0:T(8,128)(2,1)S(1)}, bf16[288,2048]{1,0:T(8,128)(2,1)S(1)}, u32[]{:S(2)}, u32[]{:S(2)}) collective-permute-start(bf16[288,2048]{1,0:T(8,128)(2,1)S(1)} %shard_map.201), channel_id=1, source_target_pairs={{0,1},{1,0},{2,3},{3,2},{4,5},{5,4},{6,7},{7,6},{8,9},{9,8},{10,11... | collective-permute-start | bytes 3538952 | tf_op jit(solution)/shard_map/ppermute | solution.py:418
  19.7 6.5 %collective-permute-start.2 = (bf16[96,2048]{1,0:T(8,128)(2,1)S(1)}, bf16[96,2048]{1,0:T(8,128)(2,1)S(1)}, u32[]{:S(2)}, u32[]{:S(2)}) collective-permute-start(bf16[96,2048]{1,0:T(8,128)(2,1)S(1)} %shard_map.199.normed.b0), channel_id=1, source_target_pairs={{0,4},{1,5},{2,6},{3,7},{4,0},{5,1},{6,2},{7,3},{8,12},{9,13},{10,... | collective-permute-start | bytes 1179656 | tf_op jit(solution)/shard_map/ppermute | solution.py:418
  26.2 9.5 %collective-permute-done.2.b3 = bf16[96,2048]{1,0:T(8,128)(2,1)S(1)} collective-permute-done((bf16[96,2048]{1,0:T(8,128)(2,1)S(1)}, bf16[96,2048]{1,0:T(8,128)(2,1)S(1)}, u32[]{:S(2)}, u32[]{:S(2)}) %collective-permute-start.2) | collective-permute-done | bytes 393248 | tf_op jit(solution)/shard_map/ppermute | solution.py:418
  35.7 2.5 %collective-permute-start.4 = (bf16[96,2048]{1,0:T(8,128)(2,1)S(1)}, bf16[96,2048]{1,0:T(8,128)(2,1)S(1)}, u32[]{:S(2)}, u32[]{:S(2)}) collective-permute-start(bf16[96,2048]{1,0:T(8,128)(2,1)S(1)} %collective-permute-done.2.b3), channel_id=1, source_target_pairs={{0,1},{1,0},{2,3},{3,2},{4,5},{5,4},{6,7},{7,6},{8,9},{9,8},{10,11... | collective-permute-start | bytes 1179656 | tf_op jit(solution)/shard_map/ppermute | solution.py:418
  38.2 2.2 %collective-permute-start.5 = (bf16[256,2048]{1,0:T(8,128)(2,1)S(1)}, bf16[256,2048]{1,0:T(8,128)(2,1)S(1)}, u32[]{:S(2)}, u32[]{:S(2)}) collective-permute-start(bf16[256,2048]{1,0:T(8,128)(2,1)S(1)} %get-tuple-element.50.w0), channel_id=1, source_target_pairs={{0,2},{1,3},{2,4},{3,5},{4,6},{5,7},{6,0},{7,1},{8,10},{9,11},{10,... | collective-permute-start | bytes 3145736 | tf_op jit(solution)/shard_map/ppermute | solution.py:418
  40.4 3.1 %collective-permute-start.6 = (bf16[256,2048]{1,0:T(8,128)(2,1)S(1)}, bf16[256,2048]{1,0:T(8,128)(2,1)}, u32[]{:S(2)}, u32[]{:S(2)}) collective-permute-start(bf16[256,2048]{1,0:T(8,128)(2,1)S(1)} %get-tuple-element.50.w0), channel_id=1, source_target_pairs={{0,6},{1,7},{2,0},{3,1},{4,2},{5,3},{6,4},{7,5},{8,14},{9,15},{10,... | collective-permute-start | bytes 3145736 | tf_op jit(solution)/shard_map/ppermute | solution.py:418
  43.5 0.0 copy-done
  43.5 4.9 %collective-permute-start.7 = (bf16[256,2048]{1,0:T(8,128)(2,1)S(1)}, bf16[256,2048]{1,0:T(8,128)(2,1)}, u32[]{:S(2)}, u32[]{:S(2)}) collective-permute-start(bf16[256,2048]{1,0:T(8,128)(2,1)S(1)} %get-tuple-element.50.w0), channel_id=1, source_target_pairs={{0,4},{1,5},{2,6},{3,7},{4,0},{5,1},{6,2},{7,3},{8,12},{9,13},{10,... | collective-permute-start | bytes 3145736 | tf_op jit(solution)/shard_map/ppermute | solution.py:418
  48.4 0.0 collective-permute-done.4.b7
  48.4 0.0 collective-permute-done.3.twins
  48.4 3.7 %shard_map.202 = (bf16[8,72,128]{2,1,0:T(8,128)(2,1)}, bf16[768,256]{1,0:T(8,128)(2,1)}, f32[8,128]{1,0:T(8,128)}, bf16[768,2048]{1,0:T(8,128)(2,1)}) custom-call(bf16[96,2048]{1,0:T(8,128)(2,1)S(1)} %shard_map.199.normed.b0, bf16[96,2048]{1,0:T(8,128)(2,1)S(1)} %collective-permute-done.b1, bf16[96,2048]{1,0:T(8,128)(2,1)S(1)} %collective-permute-done.1.b2, ...), custom_call_target="tpu_custom_call" | custom-call | flops 100000000 | bytes 1048576 | tf_op jit(solution)/shard_map/pallas_call | solution.py:28
  52.1 6.7 %all-to-all-start = ((bf16[8,72,128]{2,1,0:T(8,128)(2,1)}), bf16[8,72,128]{2,1,0:T(8,128)(2,1)S(1)}, u32[]{:S(2)}, u32[]{:S(2)}) async-start(bf16[8,72,128]{2,1,0:T(8,128)(2,1)} %get-tuple-element.34), calls=%async_computation | async-start | bytes 294912 | tf_op jit(solution)/shard_map/all_to_all | solution.py:422
  58.8 3.4 %shard_map.203 = (bf16[768,128]{1,0:T(8,128)(2,1)}, f32[128,128]{1,0:T(8,128)}) custom-call(f32[8,128]{1,0:T(8,128)} %get-tuple-element.35.level_in, bf16[768,256]{1,0:T(8,128)(2,1)} %get-tuple-element.36.kqv.kqv_in), custom_call_target="tpu_custom_call" | custom-call | flops 1000000000 | bytes 1048576 | tf_op jit(solution)/shard_map/pallas_call | solution.py:28
  62.2 0.0 all-to-all-done.received
  62.2 0.9 shard_map.204
  63.1 12.7 %all-to-all-start.1 = ((bf16[8,72,128]{2,1,0:T(8,128)(2,1)}), bf16[8,72,128]{2,1,0:T(8,128)(2,1)S(1)}, u32[]{:S(2)}, u32[]{:S(2)}) async-start(bf16[8,72,128]{2,1,0:T(8,128)(2,1)} %get-tuple-element.38), calls=%async_computation.1 | async-start | bytes 294912 | tf_op jit(solution)/shard_map/all_to_all | solution.py:422
  75.8 4.4 %shard_map.205 = (bf16[768,128]{1,0:T(8,128)(2,1)S(1)}, bf16[768,128]{1,0:T(8,128)(2,1)S(1)}, f32[32,128]{1,0:T(8,128)S(1)}, f32[72,128]{1,0:T(8,128)S(1)}, f32[...) custom-call(bf16[768,2048]{1,0:T(8,128)(2,1)} %get-tuple-element.39.row, ...), custom_call_target="tpu_custom_call" | custom-call | flops 1000000000 | bytes 1048576 | tf_op jit(solution)/shard_map/pallas_call | solution.py:28
  80.3 0.0 all-to-all-done.1.received
  80.3 1.6 %shard_map.206 = bf16[768,256]{1,0:T(8,128)(2,1)} custom-call(bf16[8,72,128]{2,1,0:T(8,128)(2,1)S(1)} %all-to-all-done.1.received, f32[48,128]{1,0:T(8,128)S(1)} %get-tuple-element.29.aside, bf16[768,128]{1,0:T(8,128)(2,1)S(1)} %get-tuple-element.42.out_gate, bf16[768,128]{1,0:T(8,128)(2,1)S(1)} %get-tuple-element.43.conv, ...), custom_call_target="tpu_custom_call" | custom-call | flops 100000000 | bytes 1048576 | tf_op jit(solution)/shard_map/pallas_call | solution.py:28
  81.9 4.2 %all-to-all-start.2 = ((bf16[4,192,256]{2,1,0:T(8,128)(2,1)}), bf16[4,192,256]{2,1,0:T(8,128)(2,1)S(1)}, u32[]{:S(2)}, u32[]{:S(2)}) async-start(bf16[4,192,256]{2,1,0:T(8,128)(2,1)} %bitcast.5), calls=%async_computation.2 | async-start | bytes 786432 | tf_op jit(solution)/shard_map/all_to_all | solution.py:516
  86.1 0.0 collective-permute-done.5.w1
  86.1 0.0 collective-permute-done.6.w2
  86.1 5.9 %collective-permute-done.7.w3 = bf16[256,2048]{1,0:T(8,128)(2,1)} collective-permute-done((bf16[256,2048]{1,0:T(8,128)(2,1)S(1)}, bf16[256,2048]{1,0:T(8,128)(2,1)}, u32[]{:S(2)}, u32[]{:S(2)}) %collective-permute-start.7) | collective-permute-done | bytes 1048608 | tf_op jit(solution)/shard_map/ppermute | solution.py:418
  92.0 4.1 %all-to-all-done.2.received = bf16[4,192,256]{2,1,0:T(8,128)(2,1)S(1)} async-done(((bf16[4,192,256]{2,1,0:T(8,128)(2,1)}), bf16[4,192,256]{2,1,0:T(8,128)(2,1)S(1)}, u32[]{:S(2)}, u32[]{:S(2)}) %all-to-all-start.2) | async-done | bytes 393248 | tf_op jit(solution)/shard_map/all_to_all | solution.py:516
  96.1 2.7 %shard_map.207 = (bf16[96,2048]{1,0:T(8,128)(2,1)S(1)}, f32[96,2048]{1,0:T(8,128)S(1)}) custom-call(bf16[4,192,256]{2,1,0:T(8,128)(2,1)S(1)} %all-to-all-done.2.received, bf16[256,2048]{1,0:T(8,128)(2,1)} %copy-done, bf16[256,2048]{1,0:T(8,128)(2,1)S(1)} %collective-permute-done.5.w1, bf16[256,2048]{1,0:T(8,128)(2,1)} %collective-permute-done.6.w2, ...), custom_call_target="tpu_custom_call" | custom-call | flops 100000000 | bytes 1048576 | tf_op jit(solution)/shard_map/pallas_call | solution.py:28
  98.9 3.1 %collective-permute-start.8 = (bf16[96,2048]{1,0:T(8,128)(2,1)S(1)}, bf16[96,2048]{1,0:T(8,128)(2,1)S(1)}, u32[]{:S(2)}, u32[]{:S(2)}) collective-permute-start(bf16[96,2048]{1,0:T(8,128)(2,1)S(1)} %get-tuple-element.52), channel_id=1, source_target_pairs={{0,1},{1,0},{2,3},{3,2},{4,5},{5,4},{6,7},{7,6},{8,9},{9,8},{10,11... | collective-permute-start | bytes 1179656 | tf_op jit(solution)/shard_map/ppermute | solution.py:418
  101.9 1.3 %collective-permute-done.8.other = bf16[96,2048]{1,0:T(8,128)(2,1)S(1)} collective-permute-done((bf16[96,2048]{1,0:T(8,128)(2,1)S(1)}, bf16[96,2048]{1,0:T(8,128)(2,1)S(1)}, u32[]{:S(2)}, u32[]{:S(2)}) %collective-permute-start.8) | collective-permute-done | bytes 393248 | tf_op jit(solution)/shard_map/ppermute | solution.py:418
  103.3 0.8 shard_map.208
Async XLA Ops:
  1.2 10.9 %collective-permute-start = (bf16[96,2048]{1,0:T(8,128)(2,1)S(1)}, bf16[96,2048]{1,0:T(8,128)(2,1)S(1)}, u32[]{:S(2)}, u32[]{:S(2)}) collective-permute-start(bf16[96,2048]{1,0:T(8,128)(2,1)S(1)} %shard_map.199.normed.b0), channel_id=1, source_target_pairs={{0,2},{1,3},{2,4},{3,5},{4,6},{5,7},{6,0},{7,1},{8,10},{9,11},{10,... | collective-permute-start | bytes 1179656 | tf_op jit(solution)/shard_map/ppermute | solution.py:418
  4.3 11.6 %collective-permute-start.1 = (bf16[96,2048]{1,0:T(8,128)(2,1)S(1)}, bf16[96,2048]{1,0:T(8,128)(2,1)S(1)}, u32[]{:S(2)}, u32[]{:S(2)}) collective-permute-start(bf16[96,2048]{1,0:T(8,128)(2,1)S(1)} %shard_map.199.normed.b0), channel_id=1, source_target_pairs={{0,6},{1,7},{2,0},{3,1},{4,2},{5,3},{6,4},{7,5},{8,14},{9,15},{10,... | collective-permute-start | bytes 1179656 | tf_op jit(solution)/shard_map/ppermute | solution.py:418
  9.3 34.2 %copy-start = (bf16[256,2048]{1,0:T(8,128)(2,1)}, bf16[256,2048]{1,0:T(8,128)(2,1)S(1)}, u32[]{:S(2)}) copy-start(bf16[256,2048]{1,0:T(8,128)(2,1)S(1)} %get-tuple-element.50.w0) | copy-start | bytes 3145732
  16.0 32.4 %collective-permute-start.3 = (bf16[288,2048]{1,0:T(8,128)(2,1)S(1)}, bf16[288,2048]{1,0:T(8,128)(2,1)S(1)}, u32[]{:S(2)}, u32[]{:S(2)}) collective-permute-start(bf16[288,2048]{1,0:T(8,128)(2,1)S(1)} %shard_map.201), channel_id=1, source_target_pairs={{0,1},{1,0},{2,3},{3,2},{4,5},{5,4},{6,7},{7,6},{8,9},{9,8},{10,11... | collective-permute-start | bytes 3538952 | tf_op jit(solution)/shard_map/ppermute | solution.py:418
  19.7 16.0 %collective-permute-start.2 = (bf16[96,2048]{1,0:T(8,128)(2,1)S(1)}, bf16[96,2048]{1,0:T(8,128)(2,1)S(1)}, u32[]{:S(2)}, u32[]{:S(2)}) collective-permute-start(bf16[96,2048]{1,0:T(8,128)(2,1)S(1)} %shard_map.199.normed.b0), channel_id=1, source_target_pairs={{0,4},{1,5},{2,6},{3,7},{4,0},{5,1},{6,2},{7,3},{8,12},{9,13},{10,... | collective-permute-start | bytes 1179656 | tf_op jit(solution)/shard_map/ppermute | solution.py:418
  35.7 12.7 %collective-permute-start.4 = (bf16[96,2048]{1,0:T(8,128)(2,1)S(1)}, bf16[96,2048]{1,0:T(8,128)(2,1)S(1)}, u32[]{:S(2)}, u32[]{:S(2)}) collective-permute-start(bf16[96,2048]{1,0:T(8,128)(2,1)S(1)} %collective-permute-done.2.b3), channel_id=1, source_target_pairs={{0,1},{1,0},{2,3},{3,2},{4,5},{5,4},{6,7},{7,6},{8,9},{9,8},{10,11... | collective-permute-start | bytes 1179656 | tf_op jit(solution)/shard_map/ppermute | solution.py:418
  38.2 47.9 %collective-permute-start.5 = (bf16[256,2048]{1,0:T(8,128)(2,1)S(1)}, bf16[256,2048]{1,0:T(8,128)(2,1)S(1)}, u32[]{:S(2)}, u32[]{:S(2)}) collective-permute-start(bf16[256,2048]{1,0:T(8,128)(2,1)S(1)} %get-tuple-element.50.w0), channel_id=1, source_target_pairs={{0,2},{1,3},{2,4},{3,5},{4,6},{5,7},{6,0},{7,1},{8,10},{9,11},{10,... | collective-permute-start | bytes 3145736 | tf_op jit(solution)/shard_map/ppermute | solution.py:418
  40.4 45.7 %collective-permute-start.6 = (bf16[256,2048]{1,0:T(8,128)(2,1)S(1)}, bf16[256,2048]{1,0:T(8,128)(2,1)}, u32[]{:S(2)}, u32[]{:S(2)}) collective-permute-start(bf16[256,2048]{1,0:T(8,128)(2,1)S(1)} %get-tuple-element.50.w0), channel_id=1, source_target_pairs={{0,6},{1,7},{2,0},{3,1},{4,2},{5,3},{6,4},{7,5},{8,14},{9,15},{10,... | collective-permute-start | bytes 3145736 | tf_op jit(solution)/shard_map/ppermute | solution.py:418
  43.5 48.5 %collective-permute-start.7 = (bf16[256,2048]{1,0:T(8,128)(2,1)S(1)}, bf16[256,2048]{1,0:T(8,128)(2,1)}, u32[]{:S(2)}, u32[]{:S(2)}) collective-permute-start(bf16[256,2048]{1,0:T(8,128)(2,1)S(1)} %get-tuple-element.50.w0), channel_id=1, source_target_pairs={{0,4},{1,5},{2,6},{3,7},{4,0},{5,1},{6,2},{7,3},{8,12},{9,13},{10,... | collective-permute-start | bytes 3145736 | tf_op jit(solution)/shard_map/ppermute | solution.py:418
  52.1 10.1 %all-to-all-start = ((bf16[8,72,128]{2,1,0:T(8,128)(2,1)}), bf16[8,72,128]{2,1,0:T(8,128)(2,1)S(1)}, u32[]{:S(2)}, u32[]{:S(2)}) async-start(bf16[8,72,128]{2,1,0:T(8,128)(2,1)} %get-tuple-element.34), calls=%async_computation | async-start | bytes 294912 | tf_op jit(solution)/shard_map/all_to_all | solution.py:422
  63.1 17.2 %all-to-all-start.1 = ((bf16[8,72,128]{2,1,0:T(8,128)(2,1)}), bf16[8,72,128]{2,1,0:T(8,128)(2,1)S(1)}, u32[]{:S(2)}, u32[]{:S(2)}) async-start(bf16[8,72,128]{2,1,0:T(8,128)(2,1)} %get-tuple-element.38), calls=%async_computation.1 | async-start | bytes 294912 | tf_op jit(solution)/shard_map/all_to_all | solution.py:422
  81.9 14.2 %all-to-all-start.2 = ((bf16[4,192,256]{2,1,0:T(8,128)(2,1)}), bf16[4,192,256]{2,1,0:T(8,128)(2,1)S(1)}, u32[]{:S(2)}, u32[]{:S(2)}) async-start(bf16[4,192,256]{2,1,0:T(8,128)(2,1)} %bitcast.5), calls=%async_computation.2 | async-start | bytes 786432 | tf_op jit(solution)/shard_map/all_to_all | solution.py:516
  98.9 4.4 %collective-permute-start.8 = (bf16[96,2048]{1,0:T(8,128)(2,1)S(1)}, bf16[96,2048]{1,0:T(8,128)(2,1)S(1)}, u32[]{:S(2)}, u32[]{:S(2)}) collective-permute-start(bf16[96,2048]{1,0:T(8,128)(2,1)S(1)} %get-tuple-element.52), channel_id=1, source_target_pairs={{0,1},{1,0},{2,3},{3,2},{4,5},{5,4},{6,7},{7,6},{8,9},{9,8},{10,11... | collective-permute-start | bytes 1179656 | tf_op jit(solution)/shard_map/ppermute | solution.py:418

commit v2 on v1

--- a/solution.py
+++ b/solution.py
@@ -114,9 +114,10 @@
 
 
 def prepare_body(
-    in_bias, forget_bias, start_scale, normed, w_key, w_query, w_input, w_forget, w_value,
-    w_inner, w_signal, w_conv, w_memory, factor, extra, taps, gain,
-    w_turned, w_value_out, w_rim, w_out, aside, sems,
+    normed, in_bias_in, forget_bias_in, start_scale_in, w_key, w_query, w_input, w_forget, w_value,
+    w_inner, w_signal, w_conv, w_memory, factor_in, extra_in, taps_in, gain_in,
+    w_turned, w_value_out, w_rim, w_out, aside,
+    in_bias, forget_bias, start_scale, factor, extra, taps, gain, sems,
 ):
     loads = [
         (w_key, w_turned.at[0:64, :]),
@@ -128,11 +129,20 @@
         (w_signal, w_rim.at[:, 128:256]),
         (w_conv, w_out.at[0:128, :]),
         (w_memory, w_out.at[128:256, :]),
+        (in_bias_in, in_bias),
+        (forget_bias_in, forget_bias),
+        (start_scale_in, start_scale),
+        (factor_in, factor),
+        (extra_in, extra),
+        (taps_in, taps),
+        (gain_in, gain),
     ]
     loads = [pltpu.make_async_copy(a, b, sems.at[i]) for i, (a, b) in enumerate(loads)]
     for load in loads:
         load.start()
     head = own_tp()
+    for load in loads[9:]:
+        load.wait()
     w_turned[144:256, :] = jnp.zeros((112, 2048), BF16)
     aside[0:8, :] = rows_of(factor[...].reshape(1, 768))
     aside[8:16, :] = rows_of(extra[pl.ds(head, 1), :])
@@ -147,7 +157,7 @@
     aside[40:48, :] = jnp.concatenate(
         [taps[:, lanes].astype(F32), own_gain, jnp.zeros((4, 128), F32)], axis=0
     )
-    for load in loads:
+    for load in loads[0:9]:
         load.wait()
 
 
@@ -345,8 +355,10 @@
         remote = dot(kqv[here, DQK : 2 * DQK], state)
         number = bring[:, b : b + 1] * remote + keep[:, b : b + 1] * local[here, :].astype(F32)
         spread = lax.rsqrt(jnp.mean(number * number, axis=1, keepdims=True) + EPS)
-        out[here, 128:256] = (number * spread * scale * out_gate[here, :].astype(F32)).astype(BF16)
-    out[:, 0:128] = conv[...]
+        there = slice(128 * ((b + 3) % 6), 128 * ((b + 3) % 6) + 128)
+        out[there, 128:256] = (number * spread * scale * out_gate[here, :].astype(F32)).astype(BF16)
+    out[384:768, 0:128] = conv[0:384, :]
+    out[0:384, 0:128] = conv[384:768, :]
     rim = before[66:70, :]
     for i in range(7):
         rim = jnp.where(jnp.logical_and(y == 0, z == i + 1), rims[i], rim)
@@ -356,7 +368,7 @@
         [tap[0:1] * past[0:1] + tap[1:2] * past[1:2], tap[0:1] * past[1:2], jnp.zeros((14, 128), F32)],
         axis=0,
     )
-    out[0:16, 0:128] = (edge[16:32, :] * (edge[0:16, :] + extra)).astype(BF16)
+    out[384:400, 0:128] = (edge[16:32, :] * (edge[0:16, :] + extra)).astype(BF16)
 
 
 def project_body(received, w0, w1, w2, w3, sent, kept, weights, sems):
@@ -377,12 +389,12 @@
     here = pl.ds(pl.multiple_of(core * 96, 32), 96)
     both = jnp.concatenate(
         [
-            jnp.concatenate([received[(x + shift) % 4, rows, :] for shift in (0, 1, 2)], axis=1)
+            jnp.concatenate([received[(x + shift + 2) % 4, rows, :] for shift in (0, 1, 2)], axis=1)
             for rows in (there, here)
         ],
         axis=0,
     )
-    low = jnp.concatenate([received[(x + 3) % 4, rows, :] for rows in (there, here)], axis=0)
+    low = jnp.concatenate([received[(x + 1) % 4, rows, :] for rows in (there, here)], axis=0)
     for n in range(4):
         for load in loads[3 * n : 3 * n + 3]:
             load.wait()
@@ -408,7 +420,7 @@
 DOWN = tp_moves(lambda x, c: (x - 1, c))
 ACROSS = tp_moves(lambda x, c: (x + 2, c))
 SWAP = tp_moves(lambda x, c: (x, 1 - c))
-X_GROUPS = [[0, 2, 4, 6], [1, 3, 5, 7]]
+X_GROUPS = [[4, 6, 0, 2], [5, 7, 1, 3]]
 TURN = (4, 5, 6, 7, 0, 1, 2, 3)
 Y_GROUPS = [[z * 8 + y for y in TURN] for z in range(8)]
 Z_GROUPS = [[z * 8 + y for z in TURN] for y in range(8)]
@@ -439,12 +451,20 @@
             ("vmem", (256, 2048), BF16),
             ("vmem", (48, 128), F32),
         ],
-        tag("smem", in_bias, forget_bias, start_scale)
-        + tag("vmem", normed)
+        tag("vmem", normed)
+        + tag("hbm", in_bias, forget_bias, start_scale)
         + tag("hbm", w_key.T, w_query.T, w_input.T, w_forget.T, w_value, w_inner, w_signal)
-        + tag("hbm", w_conv_out, w_memory_out)
-        + tag("load", factor, extra.T, taps, head_gain),
-        [pltpu.SemaphoreType.DMA((9,))],
+        + tag("hbm", w_conv_out, w_memory_out, factor, extra.T, taps, head_gain),
+        [
+            pltpu.SMEM((8,), F32),
+            pltpu.SMEM((8,), F32),
+            pltpu.SMEM((8,), F32),
+            pltpu.VMEM((768,), F32),
+            pltpu.VMEM((8, 768), F32),
+            pltpu.VMEM((3, 1024), BF16),
+            pltpu.VMEM((1024,), BF16),
+            pltpu.SemaphoreType.DMA((16,)),
+        ],
     )
     low = move(normed, UP)
     far = move(normed, ACROSS)

time: 105 us -> 105 us (level)
  no operation moved by 1% of the time
where the time goes in v2:
time: 105 us; the launch traced here: 104 us
  starting transfers between devices  54.6 us (52%)
  waiting for transfers between devices  28.3 us (27%)
  Pallas kernels  21 us (20%)
    ppermute x9, starting transfers between devices, move(): return lax.ppermute(value, 'tp', pairs)  31.2 us
    ppermute x9, waiting for transfers between devices, move(): return lax.ppermute(value, 'tp', pairs)  24.2 us
    pallas_call x10, Pallas kernels, call(): pl.pallas_call(body, out_shape=tuple((SPACES[how][0](shape, kind) for how...  21 us
    all_to_all x2, starting transfers between devices, to_all(): return lax.all_to_all(copies, 'sp', 0, 0, axis_index_groups=groups)  19.4 us
    all_to_all x1, waiting for transfers between devices, on_device(): lax.all_to_all(both.reshape(4, 192, 256), 'tp', 0, 0, axis_index_groups=X...  4.11 us
    all_to_all x1, starting transfers between devices, on_device(): lax.all_to_all(both.reshape(4, 192, 256), 'tp', 0, 0, axis_index_groups=X...  4.05 us
  transfers between devices with their start and end apart: 12, of which 6 were waited for; matrix products, arithmetic and copies ran while one was open for 0% of the time, Pallas kernels for 16%

profile of v2, /device:TPU:3, one launch (start us, length us, event | category | flops | bytes accessed | tf_op | source)
XLA Modules:
  0.0 104.1 jit_solution(12502611944133878458)
XLA Ops:
  0.0 1.2 %shard_map.199.normed.b0 = bf16[96,2048]{1,0:T(8,128)(2,1)S(1)} custom-call(bf16[96,2048]{1,0:T(8,128)(2,1)} %tokens.1, bf16[2048]{0:T(1024)(128)(2,1)} %gain.1), custom_call_target="tpu_custom_call" | custom-call | flops 100000000 | bytes 1048576 | tf_op jit(solution)/shard_map/pallas_call | solution.py:28
  1.2 3.1 %collective-permute-start = (bf16[96,2048]{1,0:T(8,128)(2,1)S(1)}, bf16[96,2048]{1,0:T(8,128)(2,1)S(1)}, u32[]{:S(2)}, u32[]{:S(2)}) collective-permute-start(bf16[96,2048]{1,0:T(8,128)(2,1)S(1)} %shard_map.199.normed.b0), channel_id=1, source_target_pairs={{0,2},{1,3},{2,4},{3,5},{4,6},{5,7},{6,0},{7,1},{8,10},{9,11},{10,... | collective-permute-start | bytes 1179656 | tf_op jit(solution)/shard_map/ppermute | solution.py:430
  4.3 2.2 %collective-permute-start.1 = (bf16[96,2048]{1,0:T(8,128)(2,1)S(1)}, bf16[96,2048]{1,0:T(8,128)(2,1)S(1)}, u32[]{:S(2)}, u32[]{:S(2)}) collective-permute-start(bf16[96,2048]{1,0:T(8,128)(2,1)S(1)} %shard_map.199.normed.b0), channel_id=1, source_target_pairs={{0,6},{1,7},{2,0},{3,1},{4,2},{5,3},{6,4},{7,5},{8,14},{9,15},{10,... | collective-permute-start | bytes 1179656 | tf_op jit(solution)/shard_map/ppermute | solution.py:430
  6.5 2.1 %shard_map.200 = (bf16[256,2048]{1,0:T(8,128)(2,1)S(1)}, bf16[2048,128]{1,0:T(8,128)(2,1)S(1)}, bf16[2048,256]{1,0:T(8,128)(2,1)S(1)}, bf16[256,2048]{1,0:T(8,128)(2,1)S(1)}, f32[48,128]{1,0:T(8,128)S(1)}) custom-call(bf16[96,2048]{1,0:T(8,128)(2,1)S(1)} %shard_map.199.normed.b0, f32[8]{0:T(128)} %in_bias_in.1, f32[8]{0:T(128)} %forget_bias_in.1, ...), custom_call_target="tpu_custom_call" | custom-call | flops 100000000 | bytes 1048576 | tf_op jit(solution)/shard_map/pallas_call | solution.py:28
  8.6 0.0 copy-start
  8.6 3.5 %collective-permute-done.b1 = bf16[96,2048]{1,0:T(8,128)(2,1)S(1)} collective-permute-done((bf16[96,2048]{1,0:T(8,128)(2,1)S(1)}, bf16[96,2048]{1,0:T(8,128)(2,1)S(1)}, u32[]{:S(2)}, u32[]{:S(2)}) %collective-permute-start) | collective-permute-done | bytes 393248 | tf_op jit(solution)/shard_map/ppermute | solution.py:430
  12.1 3.8 %collective-permute-done.1.b2 = bf16[96,2048]{1,0:T(8,128)(2,1)S(1)} collective-permute-done((bf16[96,2048]{1,0:T(8,128)(2,1)S(1)}, bf16[96,2048]{1,0:T(8,128)(2,1)S(1)}, u32[]{:S(2)}, u32[]{:S(2)}) %collective-permute-start.1) | collective-permute-done | bytes 393248 | tf_op jit(solution)/shard_map/ppermute | solution.py:430
  15.9 0.1 shard_map.201
  16.0 3.7 %collective-permute-start.3 = (bf16[288,2048]{1,0:T(8,128)(2,1)S(1)}, bf16[288,2048]{1,0:T(8,128)(2,1)S(1)}, u32[]{:S(2)}, u32[]{:S(2)}) collective-permute-start(bf16[288,2048]{1,0:T(8,128)(2,1)S(1)} %shard_map.201), channel_id=1, source_target_pairs={{0,1},{1,0},{2,3},{3,2},{4,5},{5,4},{6,7},{7,6},{8,9},{9,8},{10,11... | collective-permute-start | bytes 3538952 | tf_op jit(solution)/shard_map/ppermute | solution.py:430
  19.7 6.5 %collective-permute-start.2 = (bf16[96,2048]{1,0:T(8,128)(2,1)S(1)}, bf16[96,2048]{1,0:T(8,128)(2,1)S(1)}, u32[]{:S(2)}, u32[]{:S(2)}) collective-permute-start(bf16[96,2048]{1,0:T(8,128)(2,1)S(1)} %shard_map.199.normed.b0), channel_id=1, source_target_pairs={{0,4},{1,5},{2,6},{3,7},{4,0},{5,1},{6,2},{7,3},{8,12},{9,13},{10,... | collective-permute-start | bytes 1179656 | tf_op jit(solution)/shard_map/ppermute | solution.py:430
  26.2 9.5 %collective-permute-done.2.b3 = bf16[96,2048]{1,0:T(8,128)(2,1)S(1)} collective-permute-done((bf16[96,2048]{1,0:T(8,128)(2,1)S(1)}, bf16[96,2048]{1,0:T(8,128)(2,1)S(1)}, u32[]{:S(2)}, u32[]{:S(2)}) %collective-permute-start.2) | collective-permute-done | bytes 393248 | tf_op jit(solution)/shard_map/ppermute | solution.py:430
  35.7 2.5 %collective-permute-start.4 = (bf16[96,2048]{1,0:T(8,128)(2,1)S(1)}, bf16[96,2048]{1,0:T(8,128)(2,1)S(1)}, u32[]{:S(2)}, u32[]{:S(2)}) collective-permute-start(bf16[96,2048]{1,0:T(8,128)(2,1)S(1)} %collective-permute-done.2.b3), channel_id=1, source_target_pairs={{0,1},{1,0},{2,3},{3,2},{4,5},{5,4},{6,7},{7,6},{8,9},{9,8},{10,11... | collective-permute-start | bytes 1179656 | tf_op jit(solution)/shard_map/ppermute | solution.py:430
  38.2 2.2 %collective-permute-start.5 = (bf16[256,2048]{1,0:T(8,128)(2,1)S(1)}, bf16[256,2048]{1,0:T(8,128)(2,1)S(1)}, u32[]{:S(2)}, u32[]{:S(2)}) collective-permute-start(bf16[256,2048]{1,0:T(8,128)(2,1)S(1)} %get-tuple-element.50.w0), channel_id=1, source_target_pairs={{0,2},{1,3},{2,4},{3,5},{4,6},{5,7},{6,0},{7,1},{8,10},{9,11},{10,... | collective-permute-start | bytes 3145736 | tf_op jit(solution)/shard_map/ppermute | solution.py:430
  40.4 3.1 %collective-permute-start.6 = (bf16[256,2048]{1,0:T(8,128)(2,1)S(1)}, bf16[256,2048]{1,0:T(8,128)(2,1)}, u32[]{:S(2)}, u32[]{:S(2)}) collective-permute-start(bf16[256,2048]{1,0:T(8,128)(2,1)S(1)} %get-tuple-element.50.w0), channel_id=1, source_target_pairs={{0,6},{1,7},{2,0},{3,1},{4,2},{5,3},{6,4},{7,5},{8,14},{9,15},{10,... | collective-permute-start | bytes 3145736 | tf_op jit(solution)/shard_map/ppermute | solution.py:430
  43.5 0.0 copy-done
  43.5 4.9 %collective-permute-start.7 = (bf16[256,2048]{1,0:T(8,128)(2,1)S(1)}, bf16[256,2048]{1,0:T(8,128)(2,1)}, u32[]{:S(2)}, u32[]{:S(2)}) collective-permute-start(bf16[256,2048]{1,0:T(8,128)(2,1)S(1)} %get-tuple-element.50.w0), channel_id=1, source_target_pairs={{0,4},{1,5},{2,6},{3,7},{4,0},{5,1},{6,2},{7,3},{8,12},{9,13},{10,... | collective-permute-start | bytes 3145736 | tf_op jit(solution)/shard_map/ppermute | solution.py:430
  48.4 0.0 collective-permute-done.4.b7
  48.4 0.0 collective-permute-done.3.twins
  48.4 3.7 %shard_map.202 = (bf16[8,72,128]{2,1,0:T(8,128)(2,1)}, bf16[768,256]{1,0:T(8,128)(2,1)}, f32[8,128]{1,0:T(8,128)}, bf16[768,2048]{1,0:T(8,128)(2,1)}) custom-call(bf16[96,2048]{1,0:T(8,128)(2,1)S(1)} %shard_map.199.normed.b0, bf16[96,2048]{1,0:T(8,128)(2,1)S(1)} %collective-permute-done.b1, bf16[96,2048]{1,0:T(8,128)(2,1)S(1)} %collective-permute-done.1.b2, ...), custom_call_target="tpu_custom_call" | custom-call | flops 100000000 | bytes 1048576 | tf_op jit(solution)/shard_map/pallas_call | solution.py:28
  52.1 6.7 %all-to-all-start = ((bf16[8,72,128]{2,1,0:T(8,128)(2,1)}), bf16[8,72,128]{2,1,0:T(8,128)(2,1)S(1)}, u32[]{:S(2)}, u32[]{:S(2)}) async-start(bf16[8,72,128]{2,1,0:T(8,128)(2,1)} %get-tuple-element.34), calls=%async_computation | async-start | bytes 294912 | tf_op jit(solution)/shard_map/all_to_all | solution.py:434
  58.8 3.4 %shard_map.203 = (bf16[768,128]{1,0:T(8,128)(2,1)}, f32[128,128]{1,0:T(8,128)}) custom-call(f32[8,128]{1,0:T(8,128)} %get-tuple-element.35.level_in, bf16[768,256]{1,0:T(8,128)(2,1)} %get-tuple-element.36.kqv.kqv_in), custom_call_target="tpu_custom_call" | custom-call | flops 1000000000 | bytes 1048576 | tf_op jit(solution)/shard_map/pallas_call | solution.py:28
  62.2 0.0 all-to-all-done.received
  62.2 0.9 shard_map.204
  63.1 12.7 %all-to-all-start.1 = ((bf16[8,72,128]{2,1,0:T(8,128)(2,1)}), bf16[8,72,128]{2,1,0:T(8,128)(2,1)S(1)}, u32[]{:S(2)}, u32[]{:S(2)}) async-start(bf16[8,72,128]{2,1,0:T(8,128)(2,1)} %get-tuple-element.38), calls=%async_computation.1 | async-start | bytes 294912 | tf_op jit(solution)/shard_map/all_to_all | solution.py:434
  75.8 4.4 %shard_map.205 = (bf16[768,128]{1,0:T(8,128)(2,1)S(1)}, bf16[768,128]{1,0:T(8,128)(2,1)S(1)}, f32[32,128]{1,0:T(8,128)S(1)}, f32[72,128]{1,0:T(8,128)S(1)}, f32[...) custom-call(bf16[768,2048]{1,0:T(8,128)(2,1)} %get-tuple-element.39.row, ...), custom_call_target="tpu_custom_call" | custom-call | flops 1000000000 | bytes 1048576 | tf_op jit(solution)/shard_map/pallas_call | solution.py:28
  80.3 0.0 all-to-all-done.1.received
  80.3 1.6 %shard_map.206 = bf16[768,256]{1,0:T(8,128)(2,1)} custom-call(bf16[8,72,128]{2,1,0:T(8,128)(2,1)S(1)} %all-to-all-done.1.received, f32[48,128]{1,0:T(8,128)S(1)} %get-tuple-element.29.aside, bf16[768,128]{1,0:T(8,128)(2,1)S(1)} %get-tuple-element.42.out_gate, bf16[768,128]{1,0:T(8,128)(2,1)S(1)} %get-tuple-element.43.conv, ...), custom_call_target="tpu_custom_call" | custom-call | flops 100000000 | bytes 1048576 | tf_op jit(solution)/shard_map/pallas_call | solution.py:28
  81.9 4.1 %all-to-all-start.2 = ((bf16[4,192,256]{2,1,0:T(8,128)(2,1)}), bf16[4,192,256]{2,1,0:T(8,128)(2,1)S(1)}, u32[]{:S(2)}, u32[]{:S(2)}) async-start(bf16[4,192,256]{2,1,0:T(8,128)(2,1)} %bitcast.5), calls=%async_computation.2 | async-start | bytes 786432 | tf_op jit(solution)/shard_map/all_to_all | solution.py:536
  86.0 0.0 collective-permute-done.5.w1
  86.0 0.0 collective-permute-done.6.w2
  86.0 6.0 %collective-permute-done.7.w3 = bf16[256,2048]{1,0:T(8,128)(2,1)} collective-permute-done((bf16[256,2048]{1,0:T(8,128)(2,1)S(1)}, bf16[256,2048]{1,0:T(8,128)(2,1)}, u32[]{:S(2)}, u32[]{:S(2)}) %collective-permute-start.7) | collective-permute-done | bytes 1048608 | tf_op jit(solution)/shard_map/ppermute | solution.py:430
  92.0 4.1 %all-to-all-done.2.received = bf16[4,192,256]{2,1,0:T(8,128)(2,1)S(1)} async-done(((bf16[4,192,256]{2,1,0:T(8,128)(2,1)}), bf16[4,192,256]{2,1,0:T(8,128)(2,1)S(1)}, u32[]{:S(2)}, u32[]{:S(2)}) %all-to-all-start.2) | async-done | bytes 393248 | tf_op jit(solution)/shard_map/all_to_all | solution.py:536
  96.1 2.7 %shard_map.207 = (bf16[96,2048]{1,0:T(8,128)(2,1)S(1)}, f32[96,2048]{1,0:T(8,128)S(1)}) custom-call(bf16[4,192,256]{2,1,0:T(8,128)(2,1)S(1)} %all-to-all-done.2.received, bf16[256,2048]{1,0:T(8,128)(2,1)} %copy-done, bf16[256,2048]{1,0:T(8,128)(2,1)S(1)} %collective-permute-done.5.w1, bf16[256,2048]{1,0:T(8,128)(2,1)} %collective-permute-done.6.w2, ...), custom_call_target="tpu_custom_call" | custom-call | flops 100000000 | bytes 1048576 | tf_op jit(solution)/shard_map/pallas_call | solution.py:28
  98.9 3.1 %collective-permute-start.8 = (bf16[96,2048]{1,0:T(8,128)(2,1)S(1)}, bf16[96,2048]{1,0:T(8,128)(2,1)S(1)}, u32[]{:S(2)}, u32[]{:S(2)}) collective-permute-start(bf16[96,2048]{1,0:T(8,128)(2,1)S(1)} %get-tuple-element.52), channel_id=1, source_target_pairs={{0,1},{1,0},{2,3},{3,2},{4,5},{5,4},{6,7},{7,6},{8,9},{9,8},{10,11... | collective-permute-start | bytes 1179656 | tf_op jit(solution)/shard_map/ppermute | solution.py:430
  101.9 1.3 %collective-permute-done.8.other = bf16[96,2048]{1,0:T(8,128)(2,1)S(1)} collective-permute-done((bf16[96,2048]{1,0:T(8,128)(2,1)S(1)}, bf16[96,2048]{1,0:T(8,128)(2,1)S(1)}, u32[]{:S(2)}, u32[]{:S(2)}) %collective-permute-start.8) | collective-permute-done | bytes 393248 | tf_op jit(solution)/shard_map/ppermute | solution.py:430
  103.3 0.8 shard_map.208
Async XLA Ops:
  1.2 10.9 %collective-permute-start = (bf16[96,2048]{1,0:T(8,128)(2,1)S(1)}, bf16[96,2048]{1,0:T(8,128)(2,1)S(1)}, u32[]{:S(2)}, u32[]{:S(2)}) collective-permute-start(bf16[96,2048]{1,0:T(8,128)(2,1)S(1)} %shard_map.199.normed.b0), channel_id=1, source_target_pairs={{0,2},{1,3},{2,4},{3,5},{4,6},{5,7},{6,0},{7,1},{8,10},{9,11},{10,... | collective-permute-start | bytes 1179656 | tf_op jit(solution)/shard_map/ppermute | solution.py:430
  4.3 11.6 %collective-permute-start.1 = (bf16[96,2048]{1,0:T(8,128)(2,1)S(1)}, bf16[96,2048]{1,0:T(8,128)(2,1)S(1)}, u32[]{:S(2)}, u32[]{:S(2)}) collective-permute-start(bf16[96,2048]{1,0:T(8,128)(2,1)S(1)} %shard_map.199.normed.b0), channel_id=1, source_target_pairs={{0,6},{1,7},{2,0},{3,1},{4,2},{5,3},{6,4},{7,5},{8,14},{9,15},{10,... | collective-permute-start | bytes 1179656 | tf_op jit(solution)/shard_map/ppermute | solution.py:430
  8.6 34.9 %copy-start = (bf16[256,2048]{1,0:T(8,128)(2,1)}, bf16[256,2048]{1,0:T(8,128)(2,1)S(1)}, u32[]{:S(2)}) copy-start(bf16[256,2048]{1,0:T(8,128)(2,1)S(1)} %get-tuple-element.50.w0) | copy-start | bytes 3145732
  16.0 32.4 %collective-permute-start.3 = (bf16[288,2048]{1,0:T(8,128)(2,1)S(1)}, bf16[288,2048]{1,0:T(8,128)(2,1)S(1)}, u32[]{:S(2)}, u32[]{:S(2)}) collective-permute-start(bf16[288,2048]{1,0:T(8,128)(2,1)S(1)} %shard_map.201), channel_id=1, source_target_pairs={{0,1},{1,0},{2,3},{3,2},{4,5},{5,4},{6,7},{7,6},{8,9},{9,8},{10,11... | collective-permute-start | bytes 3538952 | tf_op jit(solution)/shard_map/ppermute | solution.py:430
  19.7 16.0 %collective-permute-start.2 = (bf16[96,2048]{1,0:T(8,128)(2,1)S(1)}, bf16[96,2048]{1,0:T(8,128)(2,1)S(1)}, u32[]{:S(2)}, u32[]{:S(2)}) collective-permute-start(bf16[96,2048]{1,0:T(8,128)(2,1)S(1)} %shard_map.199.normed.b0), channel_id=1, source_target_pairs={{0,4},{1,5},{2,6},{3,7},{4,0},{5,1},{6,2},{7,3},{8,12},{9,13},{10,... | collective-permute-start | bytes 1179656 | tf_op jit(solution)/shard_map/ppermute | solution.py:430
  35.7 12.7 %collective-permute-start.4 = (bf16[96,2048]{1,0:T(8,128)(2,1)S(1)}, bf16[96,2048]{1,0:T(8,128)(2,1)S(1)}, u32[]{:S(2)}, u32[]{:S(2)}) collective-permute-start(bf16[96,2048]{1,0:T(8,128)(2,1)S(1)} %collective-permute-done.2.b3), channel_id=1, source_target_pairs={{0,1},{1,0},{2,3},{3,2},{4,5},{5,4},{6,7},{7,6},{8,9},{9,8},{10,11... | collective-permute-start | bytes 1179656 | tf_op jit(solution)/shard_map/ppermute | solution.py:430
  38.2 47.8 %collective-permute-start.5 = (bf16[256,2048]{1,0:T(8,128)(2,1)S(1)}, bf16[256,2048]{1,0:T(8,128)(2,1)S(1)}, u32[]{:S(2)}, u32[]{:S(2)}) collective-permute-start(bf16[256,2048]{1,0:T(8,128)(2,1)S(1)} %get-tuple-element.50.w0), channel_id=1, source_target_pairs={{0,2},{1,3},{2,4},{3,5},{4,6},{5,7},{6,0},{7,1},{8,10},{9,11},{10,... | collective-permute-start | bytes 3145736 | tf_op jit(solution)/shard_map/ppermute | solution.py:430
  40.4 45.6 %collective-permute-start.6 = (bf16[256,2048]{1,0:T(8,128)(2,1)S(1)}, bf16[256,2048]{1,0:T(8,128)(2,1)}, u32[]{:S(2)}, u32[]{:S(2)}) collective-permute-start(bf16[256,2048]{1,0:T(8,128)(2,1)S(1)} %get-tuple-element.50.w0), channel_id=1, source_target_pairs={{0,6},{1,7},{2,0},{3,1},{4,2},{5,3},{6,4},{7,5},{8,14},{9,15},{10,... | collective-permute-start | bytes 3145736 | tf_op jit(solution)/shard_map/ppermute | solution.py:430
  43.5 48.5 %collective-permute-start.7 = (bf16[256,2048]{1,0:T(8,128)(2,1)S(1)}, bf16[256,2048]{1,0:T(8,128)(2,1)}, u32[]{:S(2)}, u32[]{:S(2)}) collective-permute-start(bf16[256,2048]{1,0:T(8,128)(2,1)S(1)} %get-tuple-element.50.w0), channel_id=1, source_target_pairs={{0,4},{1,5},{2,6},{3,7},{4,0},{5,1},{6,2},{7,3},{8,12},{9,13},{10,... | collective-permute-start | bytes 3145736 | tf_op jit(solution)/shard_map/ppermute | solution.py:430
  52.1 10.1 %all-to-all-start = ((bf16[8,72,128]{2,1,0:T(8,128)(2,1)}), bf16[8,72,128]{2,1,0:T(8,128)(2,1)S(1)}, u32[]{:S(2)}, u32[]{:S(2)}) async-start(bf16[8,72,128]{2,1,0:T(8,128)(2,1)} %get-tuple-element.34), calls=%async_computation | async-start | bytes 294912 | tf_op jit(solution)/shard_map/all_to_all | solution.py:434
  63.1 17.2 %all-to-all-start.1 = ((bf16[8,72,128]{2,1,0:T(8,128)(2,1)}), bf16[8,72,128]{2,1,0:T(8,128)(2,1)S(1)}, u32[]{:S(2)}, u32[]{:S(2)}) async-start(bf16[8,72,128]{2,1,0:T(8,128)(2,1)} %get-tuple-element.38), calls=%async_computation.1 | async-start | bytes 294912 | tf_op jit(solution)/shard_map/all_to_all | solution.py:434
  81.9 14.2 %all-to-all-start.2 = ((bf16[4,192,256]{2,1,0:T(8,128)(2,1)}), bf16[4,192,256]{2,1,0:T(8,128)(2,1)S(1)}, u32[]{:S(2)}, u32[]{:S(2)}) async-start(bf16[4,192,256]{2,1,0:T(8,128)(2,1)} %bitcast.5), calls=%async_computation.2 | async-start | bytes 786432 | tf_op jit(solution)/shard_map/all_to_all | solution.py:536
  98.9 4.4 %collective-permute-start.8 = (bf16[96,2048]{1,0:T(8,128)(2,1)S(1)}, bf16[96,2048]{1,0:T(8,128)(2,1)S(1)}, u32[]{:S(2)}, u32[]{:S(2)}) collective-permute-start(bf16[96,2048]{1,0:T(8,128)(2,1)S(1)} %get-tuple-element.52), channel_id=1, source_target_pairs={{0,1},{1,0},{2,3},{3,2},{4,5},{5,4},{6,7},{7,6},{8,9},{9,8},{10,11... | collective-permute-start | bytes 1179656 | tf_op jit(solution)/shard_map/ppermute | solution.py:430

commit v3 on v2

--- a/solution.py
+++ b/solution.py
@@ -45,7 +45,15 @@
     return lax.dot_general(a, b, (dims, ((), ())), preferred_element_type=F32)
 
 
-def norm_body(tokens, gain, out):
+def norm_body(tokens_in, gain_in, out, tokens, gain, sems):
+    loads = [
+        pltpu.make_async_copy(tokens_in, tokens, sems.at[0]),
+        pltpu.make_async_copy(gain_in, gain, sems.at[1]),
+    ]
+    for load in loads:
+        load.start()
+    for load in loads:
+        load.wait()
     wide = tokens[...].astype(F32)
     scale = lax.rsqrt(jnp.mean(wide * wide, axis=1, keepdims=True) + EPS)
     out[...] = (wide * scale * gain[...].astype(F32).reshape(1, 2048)).astype(BF16)
@@ -245,8 +253,8 @@
 
 
 def mixer_body(
-    rows_in, w_outer, w_inner, w_signal, w_gate, aside, before_in, start_state, local_in, tops_in,
-    kqv_in, gate_out, conv_out, edge_out, before, first_state, tops, local, query,
+    rows_in, w_outer, w_inner, w_signal, w_gate, aside, received, payload, start_state, local_in, tops_in,
+    kqv_in, before, gate_out, conv_out, edge_out, first_state, tops, local, query,
     rows, w_all, sems,
 ):
     loads = [
@@ -255,7 +263,6 @@
         pltpu.make_async_copy(rows_in, rows, sems.at[2]),
         pltpu.make_async_copy(w_signal, w_all.at[:, 256:384], sems.at[3]),
         pltpu.make_async_copy(w_gate, w_all.at[:, 384:512], sems.at[4]),
-        pltpu.make_async_copy(before_in, before, sems.at[5]),
         pltpu.make_async_copy(start_state.at[own_tp()], first_state, sems.at[6]),
         pltpu.make_async_copy(tops_in, tops, sems.at[7]),
         pltpu.make_async_copy(local_in, local, sems.at[8]),
@@ -263,6 +270,15 @@
     ]
     for load in loads:
         load.start()
+    me = own_sp() % 8
+    states, peaks, decays, rims = unpack(received)
+    earlier = [i < me for i in range(8)]
+    state, peak, decay = merged(states, peaks, decays, earlier, earlier)
+    rim = jnp.zeros((4, 128), F32)
+    for i in range(7):
+        rim = jnp.where(me == i + 1, rims[i], rim)
+    before[0:64, :] = state
+    before[64:72, :] = jnp.concatenate([peak, decay, rim, jnp.zeros((2, 128), F32)], axis=0)
     for load in loads[0:5]:
         load.wait()
     first = dot(rows[...], w_all[:, 0:256])
@@ -313,25 +329,17 @@
     )
 
 
-def line_body(received, tops, payload, before):
-    me = own_sp() % 8
+def line_body(received, tops, payload):
     states, peaks, decays, rims = unpack(received)
     every = [True] * 8
     state, peak, decay = merged(states, peaks, decays, every, every)
     sent = packed(state, peak, decay, rims[7])
     for i in range(8):
         payload[i] = sent
-    earlier = [i < me for i in range(8)]
-    state, peak, decay = merged(states, peaks, decays, earlier, earlier)
-    rim = jnp.zeros((4, 128), F32)
-    for i in range(7):
-        rim = jnp.where(me == i + 1, rims[i], rim)
-    before[0:64, :] = state
-    before[64:72, :] = jnp.concatenate([peak, decay, rim, jnp.zeros((2, 128), F32)], axis=0)
 
 
 def final_body(
-    received, aside, out_gate, conv, edge, before, first_state, tops, local, kqv, out
+    received, aside, before, out_gate, conv, edge, first_state, tops, local, kqv, out
 ):
     y, z = own_sp() % 8, own_sp() // 8
     states, peaks, decays, rims = unpack(received)
@@ -440,7 +448,14 @@
     w_conv_out, w_memory_out,
 ):
     normed = call(
-        norm_body, [("vmem", (96, 2048), BF16)], tag("load", tokens, input_norm_gain)
+        norm_body,
+        [("vmem", (96, 2048), BF16)],
+        tag("hbm", tokens, input_norm_gain),
+        [
+            pltpu.VMEM((96, 2048), BF16),
+            pltpu.VMEM((2048,), BF16),
+            pltpu.SemaphoreType.DMA((2,)),
+        ],
     )
     *prepared, w_out, aside = call(
         prepare_body,
@@ -500,29 +515,31 @@
         tag("load", level, kqv),
         flops=10**9,
     )
-    payload, before = call(
+    line = received
+    payload = call(
         line_body,
-        [("vmem", (8, PAYLOAD, 128), BF16), ("load", (72, 128), F32)],
-        tag("vmem", received) + tag("hbm", tops),
+        [("vmem", (8, PAYLOAD, 128), BF16)],
+        tag("vmem", line) + tag("hbm", tops),
     )
     w_far = w_out
     w_far = move(w_far, ACROSS)
     received = to_all(payload, Z_GROUPS)
-    prefetched = call(
+    before, *prefetched = call(
         mixer_body,
         [
+            ("vmem", (72, 128), F32),
             ("vmem", (768, 128), BF16),
             ("vmem", (768, 128), BF16),
             ("vmem", (32, 128), F32),
-            ("vmem", (72, 128), F32),
             ("vmem", (64, 128), F32),
             ("vmem", (128, 128), F32),
             ("vmem", (768, 128), BF16),
             ("vmem", (768, 128), BF16),
         ],
         tag("hbm", rows, w_outer, w_inner, w_signal, w_gate)
-        + tag("vmem", aside)
-        + tag("hbm", before, start_state, local, tops, kqv),
+        + tag("vmem", aside, line)
+        + tag("hbm", payload)
+        + tag("hbm", start_state, local, tops, kqv),
         [
             pltpu.VMEM((768, 2048), BF16),
             pltpu.VMEM((2048, 512), BF16),
@@ -531,7 +548,7 @@
         flops=10**9,
     )
     both = call(
-        final_body, [("vmem", (768, 256), BF16)], tag("vmem", received, aside, *prefetched)
+        final_body, [("vmem", (768, 256), BF16)], tag("vmem", received, aside, before, *prefetched)
     )
     mixers = lax.all_to_all(both.reshape(4, 192, 256), "tp", 0, 0, axis_index_groups=X_GROUPS)
     sent, kept = call(

time: 105 us -> 105 us (level)
  no operation moved by 1% of the time
where the time goes in v3:
time: 105 us; the launch traced here: 104 us
  starting transfers between devices  54.6 us (52%)
  waiting for transfers between devices  28.3 us (27%)
  Pallas kernels  21 us (20%)
    ppermute x9, starting transfers between devices, move(): return lax.ppermute(value, 'tp', pairs)  31.2 us
    ppermute x9, waiting for transfers between devices, move(): return lax.ppermute(value, 'tp', pairs)  24.2 us
    pallas_call x10, Pallas kernels, call(): pl.pallas_call(body, out_shape=tuple((SPACES[how][0](shape, kind) for how...  21 us
    all_to_all x2, starting transfers between devices, to_all(): return lax.all_to_all(copies, 'sp', 0, 0, axis_index_groups=groups)  19.4 us
    all_to_all x1, waiting for transfers between devices, on_device(): lax.all_to_all(both.reshape(4, 192, 256), 'tp', 0, 0, axis_index_groups=X...  4.11 us
    all_to_all x1, starting transfers between devices, on_device(): lax.all_to_all(both.reshape(4, 192, 256), 'tp', 0, 0, axis_index_groups=X...  4.04 us
  transfers between devices with their start and end apart: 12, of which 6 were waited for; matrix products, arithmetic and copies ran while one was open for 0% of the time, Pallas kernels for 16%

profile of v3, /device:TPU:3, one launch (start us, length us, event | category | flops | bytes accessed | tf_op | source)
XLA Modules:
  0.0 104.1 jit_solution(6853328993113038969)
XLA Ops:
  0.0 1.2 %shard_map.199.normed.b0 = bf16[96,2048]{1,0:T(8,128)(2,1)S(1)} custom-call(bf16[96,2048]{1,0:T(8,128)(2,1)} %tokens_in.1, bf16[2048]{0:T(1024)(128)(2,1)} %gain_in.2), custom_call_target="tpu_custom_call" | custom-call | flops 100000000 | bytes 1048576 | tf_op jit(solution)/shard_map/pallas_call | solution.py:28
  1.2 3.1 %collective-permute-start = (bf16[96,2048]{1,0:T(8,128)(2,1)S(1)}, bf16[96,2048]{1,0:T(8,128)(2,1)S(1)}, u32[]{:S(2)}, u32[]{:S(2)}) collective-permute-start(bf16[96,2048]{1,0:T(8,128)(2,1)S(1)} %shard_map.199.normed.b0), channel_id=1, source_target_pairs={{0,2},{1,3},{2,4},{3,5},{4,6},{5,7},{6,0},{7,1},{8,10},{9,11},{10,... | collective-permute-start | bytes 1179656 | tf_op jit(solution)/shard_map/ppermute | solution.py:438
  4.3 2.2 %collective-permute-start.1 = (bf16[96,2048]{1,0:T(8,128)(2,1)S(1)}, bf16[96,2048]{1,0:T(8,128)(2,1)S(1)}, u32[]{:S(2)}, u32[]{:S(2)}) collective-permute-start(bf16[96,2048]{1,0:T(8,128)(2,1)S(1)} %shard_map.199.normed.b0), channel_id=1, source_target_pairs={{0,6},{1,7},{2,0},{3,1},{4,2},{5,3},{6,4},{7,5},{8,14},{9,15},{10,... | collective-permute-start | bytes 1179656 | tf_op jit(solution)/shard_map/ppermute | solution.py:438
  6.5 2.1 %shard_map.200 = (bf16[256,2048]{1,0:T(8,128)(2,1)S(1)}, bf16[2048,128]{1,0:T(8,128)(2,1)S(1)}, bf16[2048,256]{1,0:T(8,128)(2,1)S(1)}, bf16[256,2048]{1,0:T(8,128)(2,1)S(1)}, f32[48,128]{1,0:T(8,128)S(1)}) custom-call(bf16[96,2048]{1,0:T(8,128)(2,1)S(1)} %shard_map.199.normed.b0, f32[8]{0:T(128)} %in_bias_in.1, f32[8]{0:T(128)} %forget_bias_in.1, ...), custom_call_target="tpu_custom_call" | custom-call | flops 100000000 | bytes 1048576 | tf_op jit(solution)/shard_map/pallas_call | solution.py:28
  8.6 0.0 copy-start
  8.6 3.5 %collective-permute-done.b1 = bf16[96,2048]{1,0:T(8,128)(2,1)S(1)} collective-permute-done((bf16[96,2048]{1,0:T(8,128)(2,1)S(1)}, bf16[96,2048]{1,0:T(8,128)(2,1)S(1)}, u32[]{:S(2)}, u32[]{:S(2)}) %collective-permute-start) | collective-permute-done | bytes 393248 | tf_op jit(solution)/shard_map/ppermute | solution.py:438
  12.1 3.8 %collective-permute-done.1.b2 = bf16[96,2048]{1,0:T(8,128)(2,1)S(1)} collective-permute-done((bf16[96,2048]{1,0:T(8,128)(2,1)S(1)}, bf16[96,2048]{1,0:T(8,128)(2,1)S(1)}, u32[]{:S(2)}, u32[]{:S(2)}) %collective-permute-start.1) | collective-permute-done | bytes 393248 | tf_op jit(solution)/shard_map/ppermute | solution.py:438
  15.9 0.1 shard_map.201
  16.0 3.7 %collective-permute-start.3 = (bf16[288,2048]{1,0:T(8,128)(2,1)S(1)}, bf16[288,2048]{1,0:T(8,128)(2,1)S(1)}, u32[]{:S(2)}, u32[]{:S(2)}) collective-permute-start(bf16[288,2048]{1,0:T(8,128)(2,1)S(1)} %shard_map.201), channel_id=1, source_target_pairs={{0,1},{1,0},{2,3},{3,2},{4,5},{5,4},{6,7},{7,6},{8,9},{9,8},{10,11... | collective-permute-start | bytes 3538952 | tf_op jit(solution)/shard_map/ppermute | solution.py:438
  19.8 6.5 %collective-permute-start.2 = (bf16[96,2048]{1,0:T(8,128)(2,1)S(1)}, bf16[96,2048]{1,0:T(8,128)(2,1)S(1)}, u32[]{:S(2)}, u32[]{:S(2)}) collective-permute-start(bf16[96,2048]{1,0:T(8,128)(2,1)S(1)} %shard_map.199.normed.b0), channel_id=1, source_target_pairs={{0,4},{1,5},{2,6},{3,7},{4,0},{5,1},{6,2},{7,3},{8,12},{9,13},{10,... | collective-permute-start | bytes 1179656 | tf_op jit(solution)/shard_map/ppermute | solution.py:438
  26.3 9.5 %collective-permute-done.2.b3 = bf16[96,2048]{1,0:T(8,128)(2,1)S(1)} collective-permute-done((bf16[96,2048]{1,0:T(8,128)(2,1)S(1)}, bf16[96,2048]{1,0:T(8,128)(2,1)S(1)}, u32[]{:S(2)}, u32[]{:S(2)}) %collective-permute-start.2) | collective-permute-done | bytes 393248 | tf_op jit(solution)/shard_map/ppermute | solution.py:438
  35.7 2.5 %collective-permute-start.4 = (bf16[96,2048]{1,0:T(8,128)(2,1)S(1)}, bf16[96,2048]{1,0:T(8,128)(2,1)S(1)}, u32[]{:S(2)}, u32[]{:S(2)}) collective-permute-start(bf16[96,2048]{1,0:T(8,128)(2,1)S(1)} %collective-permute-done.2.b3), channel_id=1, source_target_pairs={{0,1},{1,0},{2,3},{3,2},{4,5},{5,4},{6,7},{7,6},{8,9},{9,8},{10,11... | collective-permute-start | bytes 1179656 | tf_op jit(solution)/shard_map/ppermute | solution.py:438
  38.2 2.2 %collective-permute-start.5 = (bf16[256,2048]{1,0:T(8,128)(2,1)S(1)}, bf16[256,2048]{1,0:T(8,128)(2,1)S(1)}, u32[]{:S(2)}, u32[]{:S(2)}) collective-permute-start(bf16[256,2048]{1,0:T(8,128)(2,1)S(1)} %get-tuple-element.46.w0), channel_id=1, source_target_pairs={{0,2},{1,3},{2,4},{3,5},{4,6},{5,7},{6,0},{7,1},{8,10},{9,11},{10,... | collective-permute-start | bytes 3145736 | tf_op jit(solution)/shard_map/ppermute | solution.py:438
  40.4 3.1 %collective-permute-start.6 = (bf16[256,2048]{1,0:T(8,128)(2,1)S(1)}, bf16[256,2048]{1,0:T(8,128)(2,1)}, u32[]{:S(2)}, u32[]{:S(2)}) collective-permute-start(bf16[256,2048]{1,0:T(8,128)(2,1)S(1)} %get-tuple-element.46.w0), channel_id=1, source_target_pairs={{0,6},{1,7},{2,0},{3,1},{4,2},{5,3},{6,4},{7,5},{8,14},{9,15},{10,... | collective-permute-start | bytes 3145736 | tf_op jit(solution)/shard_map/ppermute | solution.py:438
  43.5 0.0 copy-done
  43.5 4.9 %collective-permute-start.7 = (bf16[256,2048]{1,0:T(8,128)(2,1)S(1)}, bf16[256,2048]{1,0:T(8,128)(2,1)}, u32[]{:S(2)}, u32[]{:S(2)}) collective-permute-start(bf16[256,2048]{1,0:T(8,128)(2,1)S(1)} %get-tuple-element.46.w0), channel_id=1, source_target_pairs={{0,4},{1,5},{2,6},{3,7},{4,0},{5,1},{6,2},{7,3},{8,12},{9,13},{10,... | collective-permute-start | bytes 3145736 | tf_op jit(solution)/shard_map/ppermute | solution.py:438
  48.4 0.0 collective-permute-done.4.b7
  48.4 0.0 collective-permute-done.3.twins
  48.4 3.7 %shard_map.202 = (bf16[8,72,128]{2,1,0:T(8,128)(2,1)}, bf16[768,256]{1,0:T(8,128)(2,1)}, f32[8,128]{1,0:T(8,128)}, bf16[768,2048]{1,0:T(8,128)(2,1)}) custom-call(bf16[96,2048]{1,0:T(8,128)(2,1)S(1)} %shard_map.199.normed.b0, bf16[96,2048]{1,0:T(8,128)(2,1)S(1)} %collective-permute-done.b1, bf16[96,2048]{1,0:T(8,128)(2,1)S(1)} %collective-permute-done.1.b2, ...), custom_call_target="tpu_custom_call" | custom-call | flops 100000000 | bytes 1048576 | tf_op jit(solution)/shard_map/pallas_call | solution.py:28
  52.2 6.7 %all-to-all-start = ((bf16[8,72,128]{2,1,0:T(8,128)(2,1)}), bf16[8,72,128]{2,1,0:T(8,128)(2,1)S(1)}, u32[]{:S(2)}, u32[]{:S(2)}) async-start(bf16[8,72,128]{2,1,0:T(8,128)(2,1)} %get-tuple-element.32), calls=%async_computation | async-start | bytes 294912 | tf_op jit(solution)/shard_map/all_to_all | solution.py:442
  58.8 3.4 %shard_map.203 = (bf16[768,128]{1,0:T(8,128)(2,1)}, f32[128,128]{1,0:T(8,128)}) custom-call(f32[8,128]{1,0:T(8,128)} %get-tuple-element.33.level_in, bf16[768,256]{1,0:T(8,128)(2,1)} %get-tuple-element.34.kqv.kqv_in), custom_call_target="tpu_custom_call" | custom-call | flops 1000000000 | bytes 1048576 | tf_op jit(solution)/shard_map/pallas_call | solution.py:28
  62.2 0.0 all-to-all-done.received
  62.2 0.9 shard_map.204.payload
  63.1 12.7 %all-to-all-start.1 = ((bf16[8,72,128]{2,1,0:T(8,128)(2,1)}), bf16[8,72,128]{2,1,0:T(8,128)(2,1)S(1)}, u32[]{:S(2)}, u32[]{:S(2)}) async-start(bf16[8,72,128]{2,1,0:T(8,128)(2,1)} %shard_map.204.payload), calls=%async_computation.1 | async-start | bytes 294912 | tf_op jit(solution)/shard_map/all_to_all | solution.py:442
  75.8 4.4 %shard_map.205 = (f32[72,128]{1,0:T(8,128)S(1)}, bf16[768,128]{1,0:T(8,128)(2,1)S(1)}, bf16[768,128]{1,0:T(8,128)(2,1)S(1)}, f32[32,128]{1,0:T(8,128)S(1)}, f32[...) custom-call(bf16[768,2048]{1,0:T(8,128)(2,1)} %get-tuple-element.36.row, ...), custom_call_target="tpu_custom_call" | custom-call | flops 1000000000 | bytes 1048576 | tf_op jit(solution)/shard_map/pallas_call | solution.py:28
  80.2 0.0 all-to-all-done.1.received
  80.3 1.6 %shard_map.206 = bf16[768,256]{1,0:T(8,128)(2,1)} custom-call(bf16[8,72,128]{2,1,0:T(8,128)(2,1)S(1)} %all-to-all-done.1.received, f32[48,128]{1,0:T(8,128)S(1)} %get-tuple-element.27.aside, f32[72,128]{1,0:T(8,128)S(1)} %get-tuple-element.38.before, bf16[768,128]{1,0:T(8,128)(2,1)S(1)} %get-tuple-element.39.out_gate, ...), custom_call_target="tpu_custom_call" | custom-call | flops 100000000 | bytes 1048576 | tf_op jit(solution)/shard_map/pallas_call | solution.py:28
  81.9 4.0 %all-to-all-start.2 = ((bf16[4,192,256]{2,1,0:T(8,128)(2,1)}), bf16[4,192,256]{2,1,0:T(8,128)(2,1)S(1)}, u32[]{:S(2)}, u32[]{:S(2)}) async-start(bf16[4,192,256]{2,1,0:T(8,128)(2,1)} %bitcast.5), calls=%async_computation.2 | async-start | bytes 786432 | tf_op jit(solution)/shard_map/all_to_all | solution.py:553
  85.9 0.0 collective-permute-done.5.w1
  85.9 0.0 collective-permute-done.6.w2
  86.0 6.1 %collective-permute-done.7.w3 = bf16[256,2048]{1,0:T(8,128)(2,1)} collective-permute-done((bf16[256,2048]{1,0:T(8,128)(2,1)S(1)}, bf16[256,2048]{1,0:T(8,128)(2,1)}, u32[]{:S(2)}, u32[]{:S(2)}) %collective-permute-start.7) | collective-permute-done | bytes 1048608 | tf_op jit(solution)/shard_map/ppermute | solution.py:438
  92.0 4.1 %all-to-all-done.2.received = bf16[4,192,256]{2,1,0:T(8,128)(2,1)S(1)} async-done(((bf16[4,192,256]{2,1,0:T(8,128)(2,1)}), bf16[4,192,256]{2,1,0:T(8,128)(2,1)S(1)}, u32[]{:S(2)}, u32[]{:S(2)}) %all-to-all-start.2) | async-done | bytes 393248 | tf_op jit(solution)/shard_map/all_to_all | solution.py:553
  96.1 2.7 %shard_map.207 = (bf16[96,2048]{1,0:T(8,128)(2,1)S(1)}, f32[96,2048]{1,0:T(8,128)S(1)}) custom-call(bf16[4,192,256]{2,1,0:T(8,128)(2,1)S(1)} %all-to-all-done.2.received, bf16[256,2048]{1,0:T(8,128)(2,1)} %copy-done, bf16[256,2048]{1,0:T(8,128)(2,1)S(1)} %collective-permute-done.5.w1, bf16[256,2048]{1,0:T(8,128)(2,1)} %collective-permute-done.6.w2, ...), custom_call_target="tpu_custom_call" | custom-call | flops 100000000 | bytes 1048576 | tf_op jit(solution)/shard_map/pallas_call | solution.py:28
  98.9 3.1 %collective-permute-start.8 = (bf16[96,2048]{1,0:T(8,128)(2,1)S(1)}, bf16[96,2048]{1,0:T(8,128)(2,1)S(1)}, u32[]{:S(2)}, u32[]{:S(2)}) collective-permute-start(bf16[96,2048]{1,0:T(8,128)(2,1)S(1)} %get-tuple-element.48), channel_id=1, source_target_pairs={{0,1},{1,0},{2,3},{3,2},{4,5},{5,4},{6,7},{7,6},{8,9},{9,8},{10,11... | collective-permute-start | bytes 1179656 | tf_op jit(solution)/shard_map/ppermute | solution.py:438
  102.0 1.3 %collective-permute-done.8.other = bf16[96,2048]{1,0:T(8,128)(2,1)S(1)} collective-permute-done((bf16[96,2048]{1,0:T(8,128)(2,1)S(1)}, bf16[96,2048]{1,0:T(8,128)(2,1)S(1)}, u32[]{:S(2)}, u32[]{:S(2)}) %collective-permute-start.8) | collective-permute-done | bytes 393248 | tf_op jit(solution)/shard_map/ppermute | solution.py:438
  103.3 0.8 shard_map.208
Async XLA Ops:
  1.2 10.9 %collective-permute-start = (bf16[96,2048]{1,0:T(8,128)(2,1)S(1)}, bf16[96,2048]{1,0:T(8,128)(2,1)S(1)}, u32[]{:S(2)}, u32[]{:S(2)}) collective-permute-start(bf16[96,2048]{1,0:T(8,128)(2,1)S(1)} %shard_map.199.normed.b0), channel_id=1, source_target_pairs={{0,2},{1,3},{2,4},{3,5},{4,6},{5,7},{6,0},{7,1},{8,10},{9,11},{10,... | collective-permute-start | bytes 1179656 | tf_op jit(solution)/shard_map/ppermute | solution.py:438
  4.3 11.6 %collective-permute-start.1 = (bf16[96,2048]{1,0:T(8,128)(2,1)S(1)}, bf16[96,2048]{1,0:T(8,128)(2,1)S(1)}, u32[]{:S(2)}, u32[]{:S(2)}) collective-permute-start(bf16[96,2048]{1,0:T(8,128)(2,1)S(1)} %shard_map.199.normed.b0), channel_id=1, source_target_pairs={{0,6},{1,7},{2,0},{3,1},{4,2},{5,3},{6,4},{7,5},{8,14},{9,15},{10,... | collective-permute-start | bytes 1179656 | tf_op jit(solution)/shard_map/ppermute | solution.py:438
  8.6 34.9 %copy-start = (bf16[256,2048]{1,0:T(8,128)(2,1)}, bf16[256,2048]{1,0:T(8,128)(2,1)S(1)}, u32[]{:S(2)}) copy-start(bf16[256,2048]{1,0:T(8,128)(2,1)S(1)} %get-tuple-element.46.w0) | copy-start | bytes 3145732
  16.0 32.4 %collective-permute-start.3 = (bf16[288,2048]{1,0:T(8,128)(2,1)S(1)}, bf16[288,2048]{1,0:T(8,128)(2,1)S(1)}, u32[]{:S(2)}, u32[]{:S(2)}) collective-permute-start(bf16[288,2048]{1,0:T(8,128)(2,1)S(1)} %shard_map.201), channel_id=1, source_target_pairs={{0,1},{1,0},{2,3},{3,2},{4,5},{5,4},{6,7},{7,6},{8,9},{9,8},{10,11... | collective-permute-start | bytes 3538952 | tf_op jit(solution)/shard_map/ppermute | solution.py:438
  19.8 16.0 %collective-permute-start.2 = (bf16[96,2048]{1,0:T(8,128)(2,1)S(1)}, bf16[96,2048]{1,0:T(8,128)(2,1)S(1)}, u32[]{:S(2)}, u32[]{:S(2)}) collective-permute-start(bf16[96,2048]{1,0:T(8,128)(2,1)S(1)} %shard_map.199.normed.b0), channel_id=1, source_target_pairs={{0,4},{1,5},{2,6},{3,7},{4,0},{5,1},{6,2},{7,3},{8,12},{9,13},{10,... | collective-permute-start | bytes 1179656 | tf_op jit(solution)/shard_map/ppermute | solution.py:438
  35.7 12.7 %collective-permute-start.4 = (bf16[96,2048]{1,0:T(8,128)(2,1)S(1)}, bf16[96,2048]{1,0:T(8,128)(2,1)S(1)}, u32[]{:S(2)}, u32[]{:S(2)}) collective-permute-start(bf16[96,2048]{1,0:T(8,128)(2,1)S(1)} %collective-permute-done.2.b3), channel_id=1, source_target_pairs={{0,1},{1,0},{2,3},{3,2},{4,5},{5,4},{6,7},{7,6},{8,9},{9,8},{10,11... | collective-permute-start | bytes 1179656 | tf_op jit(solution)/shard_map/ppermute | solution.py:438
  38.2 47.7 %collective-permute-start.5 = (bf16[256,2048]{1,0:T(8,128)(2,1)S(1)}, bf16[256,2048]{1,0:T(8,128)(2,1)S(1)}, u32[]{:S(2)}, u32[]{:S(2)}) collective-permute-start(bf16[256,2048]{1,0:T(8,128)(2,1)S(1)} %get-tuple-element.46.w0), channel_id=1, source_target_pairs={{0,2},{1,3},{2,4},{3,5},{4,6},{5,7},{6,0},{7,1},{8,10},{9,11},{10,... | collective-permute-start | bytes 3145736 | tf_op jit(solution)/shard_map/ppermute | solution.py:438
  40.4 45.5 %collective-permute-start.6 = (bf16[256,2048]{1,0:T(8,128)(2,1)S(1)}, bf16[256,2048]{1,0:T(8,128)(2,1)}, u32[]{:S(2)}, u32[]{:S(2)}) collective-permute-start(bf16[256,2048]{1,0:T(8,128)(2,1)S(1)} %get-tuple-element.46.w0), channel_id=1, source_target_pairs={{0,6},{1,7},{2,0},{3,1},{4,2},{5,3},{6,4},{7,5},{8,14},{9,15},{10,... | collective-permute-start | bytes 3145736 | tf_op jit(solution)/shard_map/ppermute | solution.py:438
  43.5 48.5 %collective-permute-start.7 = (bf16[256,2048]{1,0:T(8,128)(2,1)S(1)}, bf16[256,2048]{1,0:T(8,128)(2,1)}, u32[]{:S(2)}, u32[]{:S(2)}) collective-permute-start(bf16[256,2048]{1,0:T(8,128)(2,1)S(1)} %get-tuple-element.46.w0), channel_id=1, source_target_pairs={{0,4},{1,5},{2,6},{3,7},{4,0},{5,1},{6,2},{7,3},{8,12},{9,13},{10,... | collective-permute-start | bytes 3145736 | tf_op jit(solution)/shard_map/ppermute | solution.py:438
  52.2 10.1 %all-to-all-start = ((bf16[8,72,128]{2,1,0:T(8,128)(2,1)}), bf16[8,72,128]{2,1,0:T(8,128)(2,1)S(1)}, u32[]{:S(2)}, u32[]{:S(2)}) async-start(bf16[8,72,128]{2,1,0:T(8,128)(2,1)} %get-tuple-element.32), calls=%async_computation | async-start | bytes 294912 | tf_op jit(solution)/shard_map/all_to_all | solution.py:442
  63.1 17.2 %all-to-all-start.1 = ((bf16[8,72,128]{2,1,0:T(8,128)(2,1)}), bf16[8,72,128]{2,1,0:T(8,128)(2,1)S(1)}, u32[]{:S(2)}, u32[]{:S(2)}) async-start(bf16[8,72,128]{2,1,0:T(8,128)(2,1)} %shard_map.204.payload), calls=%async_computation.1 | async-start | bytes 294912 | tf_op jit(solution)/shard_map/all_to_all | solution.py:442
  81.9 14.2 %all-to-all-start.2 = ((bf16[4,192,256]{2,1,0:T(8,128)(2,1)}), bf16[4,192,256]{2,1,0:T(8,128)(2,1)S(1)}, u32[]{:S(2)}, u32[]{:S(2)}) async-start(bf16[4,192,256]{2,1,0:T(8,128)(2,1)} %bitcast.5), calls=%async_computation.2 | async-start | bytes 786432 | tf_op jit(solution)/shard_map/all_to_all | solution.py:553
  98.9 4.4 %collective-permute-start.8 = (bf16[96,2048]{1,0:T(8,128)(2,1)S(1)}, bf16[96,2048]{1,0:T(8,128)(2,1)S(1)}, u32[]{:S(2)}, u32[]{:S(2)}) collective-permute-start(bf16[96,2048]{1,0:T(8,128)(2,1)S(1)} %get-tuple-element.48), channel_id=1, source_target_pairs={{0,1},{1,0},{2,3},{3,2},{4,5},{5,4},{6,7},{7,6},{8,9},{9,8},{10,11... | collective-permute-start | bytes 1179656 | tf_op jit(solution)/shard_map/ppermute | solution.py:438
